TPU v7x, 768 devices: a whole 4x8x12 slice. The times are simulated.
768 devices in a mesh: sp: 16 (over y, core), dp: 48 (over z, x).
Axes of the slice: x: 4, y: 8, z: 12, core: 2. Of those that a mesh axis runs over, the one named last changes fastest.
Arguments:
- stream: bfloat16 [48, 2048, 2064], P('dp', 'sp'), may hold values from -6 to 6
- mix_gain: float32 [2064], replicated, may hold values from 0.1 to 1.9
- query_weight: bfloat16 [2064, 2048], P('dp'), may hold values from -0.125 to 0.125
- query_gain: float32 [128], replicated, may hold values from 0.1 to 1.9
- keys: bfloat16 [48, 2048, 512], P('dp', 'sp'), may hold values from -6 to 6
- key_gain: float32 [128], replicated, may hold values from 0.1 to 1.9
- values: bfloat16 [48, 2048, 512], P('dp', 'sp'), may hold values from -48 to 48
- stick_offset: float32 [16], replicated, may hold values from -8.5 to -7, as said below
Outputs:
- attended: bfloat16 [48, 2048, 2048], P('dp', 'sp')
Inputs may be any that keep to these rules, and one draw needn't show every extreme that they name: `stick_offset`: one offset for each query head, added to all of that head's scores.
All inputs are finite; a program needn't handle non-finite values.
Results may differ from a plain program's by a relative error of at most 0.012.
Values may be sent and summed in bfloat16 or wider, within the bound.
No kernel may reach another device: no remote copies, remote signals or barrier semaphores. Data moves between devices by JAX's collectives and lax.ppermute only.
A program may use at most 64 MiB of HBM per device.

v0:
```python
import math

import jax
import jax.numpy as jnp
from jax import lax
from jax.sharding import PartitionSpec as P

norm_eps = 1e-06
row_block = 256
key_block = 128


def sent_to_all(value, axis):
    copies = jnp.broadcast_to(value, (lax.axis_size(axis), *value.shape))
    return lax.all_to_all(copies, axis, split_axis=0, concat_axis=0, tiled=True)


def joined_along(pieces, dim):
    pieces = jnp.moveaxis(pieces, 0, dim)
    lengths = pieces.shape
    return pieces.reshape(*lengths[:dim], lengths[dim] * lengths[dim + 1], *lengths[dim + 2 :])


def gather_directly(value, axis, dim):
    pieces = sent_to_all(value, axis)
    return joined_along(pieces, dim)


def rms_scaled(inputs, gain):
    wide = inputs.astype(jnp.float32)
    scaled = wide * lax.rsqrt(jnp.mean(wide * wide, axis=-1, keepdims=True) + norm_eps) * gain
    return scaled.astype(jnp.bfloat16)


def stick_weights(scores, first_row):
    heads_here = scores.shape[0]
    rows_here = scores.shape[1]
    keys_here = scores.shape[2]
    width = math.gcd(keys_here, key_block)
    blocks_here = keys_here // width
    query_pos = first_row + jnp.arange(rows_here, dtype=jnp.int32)
    key_pos = jnp.arange(keys_here, dtype=jnp.int32)
    causal = key_pos[None, :] < query_pos[:, None]
    log_keep = jnp.where(causal, jax.nn.log_sigmoid(-scores), 0.0)
    pieces = log_keep.reshape(heads_here, rows_here, blocks_here, width)
    inner = jnp.arange(width, dtype=jnp.int32)
    upper = (inner[:, None] > inner[None, :]).astype(jnp.float32)
    local = jnp.einsum("hqbk,kj->hqbj", pieces, upper, precision=lax.Precision.HIGHEST)
    totals = jnp.sum(pieces, axis=3)
    later = lax.cumsum(totals, axis=2, reverse=True) - totals
    tail = (local + later[:, :, :, None]).reshape(heads_here, rows_here, keys_here)
    return jnp.where(causal, jnp.exp(jax.nn.log_sigmoid(scores) + tail), 0.0)


def body(stream, mix_gain, query_weight, query_gain, keys, key_gain, values, stick_offset):
    sp_count = lax.axis_size("sp")
    sp_index = lax.axis_index("sp")
    stream_rows = stream[0]
    tokens_dev = stream_rows.shape[0]
    head_width = query_gain.shape[0]
    heads_all = stick_offset.shape[0]
    heads_dev = heads_all // sp_count
    kv_count = keys.shape[2] // head_width
    group_size = sp_count // kv_count
    seq_length = tokens_dev * sp_count
    stacked = jnp.stack((keys[0], values[0]), axis=1).reshape(tokens_dev, 2, kv_count, head_width)
    copied = jnp.repeat(stacked, group_size, axis=2)
    arrived = lax.all_to_all(copied, "sp", split_axis=2, concat_axis=0, tiled=True)
    key_value = arrived[:, :, 0, :]
    normed = rms_scaled(stream_rows, mix_gain)
    columns = lax.dynamic_slice_in_dim(
        query_weight, sp_index * (heads_dev * head_width), heads_dev * head_width, 1
    )
    gathered = gather_directly(columns, "dp", 0)
    queries = jnp.dot(
        lax.all_gather(normed, "sp", axis=0, tiled=True),
        gathered,
        preferred_element_type=jnp.float32,
    ).astype(jnp.bfloat16)
    queries = lax.optimization_barrier(queries)
    mine = rms_scaled(queries.reshape(seq_length, heads_dev, head_width), query_gain)
    key_heads = rms_scaled(key_value[:, 0], key_gain)
    value_rows = key_value[:, 1]
    offsets = lax.dynamic_slice_in_dim(stick_offset, sp_index * heads_dev, heads_dev)
    block = math.gcd(seq_length, row_block)
    outputs = []
    for block_id in range(seq_length // block):
        first = block_id * block
        finish = first + block
        scores = jnp.einsum(
            "qhd,kd->hqk",
            mine[first:finish],
            key_heads[:finish],
            preferred_element_type=jnp.float32,
        )
        scores = scores * head_width ** (-0.5) + offsets[:, None, None]
        weights = stick_weights(scores, first).astype(jnp.bfloat16)
        outputs.append(
            jnp.einsum(
                "hqk,kd->qhd", weights, value_rows[:finish], preferred_element_type=jnp.float32
            )
        )
    attended = (
        jnp.concatenate(outputs, axis=0)
        .reshape(seq_length, heads_dev * head_width)
        .astype(jnp.bfloat16)
    )
    returned = lax.all_to_all(attended, "sp", split_axis=0, concat_axis=1, tiled=True)
    return returned[None]


def solution(mesh):
    return jax.shard_map(
        body,
        mesh=mesh,
        in_specs=(
            P("dp", "sp", None),
            P(),
            P("dp", None),
            P(),
            P("dp", "sp", None),
            P(),
            P("dp", "sp", None),
            P(),
        ),
        out_specs=P("dp", "sp", None),
        check_vma=False,
    )
```

profile of v0, /device:TPU:1, one launch (start us, length us, event | category | flops | bytes accessed | tf_op | source)
XLA Modules:
  0.0 225.5 jit_solution(712548119325259054)
XLA Ops:
  6.5 1.4 fusion.62
  7.9 2.2 fusion.64
  10.2 0.9 broadcast_in_dim.47
  11.1 18.8 %all-to-all-start.1 = ((bf16[48,43,128]{2,1,0:T(8,128)(2,1)}), bf16[48,43,128]{2,1,0:T(8,128)(2,1)S(1)}, u32[]{:S(2)}, u32[]{:S(2)}) async-start(bf16[48,43,128]{2,1,0:T(8,128)(2,1)} %broadcast_in_dim.47), calls=%async_computation.1 | async-start | bytes 1179648 | tf_op jit(solution)/shard_map/all_to_all | solution.py:15
  30.3 25.4 %all-to-all-done.1 = bf16[48,43,128]{2,1,0:T(8,128)(2,1)S(1)} async-done(((bf16[48,43,128]{2,1,0:T(8,128)(2,1)}), bf16[48,43,128]{2,1,0:T(8,128)(2,1)S(1)}, u32[]{:S(2)}, u32[]{:S(2)}) %all-to-all-start.1) | async-done | bytes 528416 | tf_op jit(solution)/shard_map/all_to_all | solution.py:15
  55.6 1.2 broadcast_in_dim.46
  56.9 10.4 %all-to-all-start = ((bf16[128,2,16,128]{3,0,1,2:T(8,128)(2,1)}), bf16[128,2,16,128]{3,0,1,2:T(8,128)(2,1)S(1)}, u32[]{:S(2)}, u32[]{:S(2)}) async-start(bf16[128,2,16,128]{3,0,1,2:T(8,128)(2,1)} %bitcast), calls=%async_computation | async-start | bytes 2097152 | tf_op jit(solution)/shard_map/all_to_all | solution.py:68
  67.3 0.6 dynamic_slice.7
  68.1 32.8 %all-to-all-done = bf16[128,2,16,128]{3,0,1,2:T(8,128)(2,1)S(1)} async-done(((bf16[128,2,16,128]{3,0,1,2:T(8,128)(2,1)}), bf16[128,2,16,128]{3,0,1,2:T(8,128)(2,1)S(1)}, u32[]{:S(2)}, u32[]{:S(2)}) %all-to-all-start) | async-done | bytes 1048608 | tf_op jit(solution)/shard_map/all_to_all | solution.py:68
  101.4 7.6 %all-gather.2.cloned.1.call-done = bf16[2048,2064]{0,1:T(8,128)(2,1)} async-done(((bf16[128,2064]{0,1:T(8,128)(2,1)}), bf16[2048,2064]{0,1:T(8,128)(2,1)}) %all-gather.2.cloned.1.call-update) | async-done | bytes 8454160 | tf_op jit(solution)/shard_map/all_gather | solution.py:76
  109.0 6.0 %convolution_convert_fusion = bf16[2048,128]{1,0:T(8,128)(2,1)S(1)} fusion(bf16[2048,2064]{0,1:T(8,128)(2,1)} %all-gather.2.cloned.1.call-done, bf16[2064,128]{1,0:T(8,128)(2,1)S(1)} %reshape.675), kind=kOutput, calls=%fused_computation.22 | convolution fusion | flops 1082392576 | bytes 9506816 | tf_op jit(solution)/shard_map/dot_general | solution.py:75
  115.3 1.4 fusion.67
  116.7 3.7 %fusion.14 = (f32[1,256,2048]{1,2,0:T(8,128)S(1)}, f32[1,256,2048]{1,2,0:T(8,128)}) fusion(s32[256]{0:T(256)S(1)} %iota_add_fusion, f32[]{:T(128)} %bitcast.10, bf16[2048,128]{1,0:T(8,128)(2,1)S(1)} %get-tuple-element.21, f32[128]{0:T(128)S(1)} %copy-done.22, f32[2048]{0:T(1024)S(1)} %add_rsqrt_fusion.1, bf16[2048,2,128]{2,0,1:T(8,128)(2,1)S(1)} %bitcast.210), kind=kOutput, calls=%fused_computation.31 | convolution fusion | flops 141033472 | bytes 4793860 | tf_op jit(solution)/shard_map/qhd,kd->hqk/dot_general | solution.py:90
  120.6 1.1 copy-done.1
  121.8 2.9 %convolution_add_fusion = f32[256,16,128]{0,2,1:T(8,128)S(1)} fusion(f32[256,16,128]{0,2,1:T(8,128)} %bitcast.220, f32[256,16]{0,1:T(8,128)S(1)} %sub.79), kind=kOutput, calls=%fused_computation.41 | convolution fusion | flops 805847040 | bytes 4210688 | tf_op jit(solution)/shard_map/hqbk,kj->hqbj/dot_general | solution.py:48
  124.7 2.6 %fusion.114 = (f32[1,256,256]{1,2,0:T(8,128)}, f32[1,256,256]{1,2,0:T(8,128)}) fusion(f32[]{:T(128)} %bitcast.10, bf16[2048,128]{1,0:T(8,128)(2,1)} %copy-done.14, bf16[2048,128]{1,0:T(8,128)(2,1)S(1)} %copy-done.15), kind=kOutput, calls=%fused_computation.171 | convolution fusion | flops 17498112 | bytes 655872 | tf_op jit(solution)/shard_map/qhd,kd->hqk/dot_general | solution.py:90
  127.2 4.7 %fusion.21 = (f32[1,256,1792]{1,2,0:T(8,128)}, f32[1,256,1792]{1,2,0:T(8,128)}) fusion(s32[256]{0:T(256)S(1)} %iota_add_fusion.1, f32[]{:T(128)} %bitcast.10, bf16[2048,128]{1,0:T(8,128)(2,1)} %copy-done.14, bf16[2048,128]{1,0:T(8,128)(2,1)S(1)} %copy-done.15), kind=kOutput, calls=%fused_computation.39 | convolution fusion | flops 122486784 | bytes 4195840 | tf_op jit(solution)/shard_map/qhd,kd->hqk/dot_general | solution.py:90
  131.9 1.6 reduce_sum.108
  133.6 3.9 %convolution_add_fusion.1 = f32[256,14,128]{0,2,1:T(8,128)} fusion(f32[256,14,128]{0,2,1:T(8,128)} %bitcast.222, f32[256,14]{0,1:T(8,128)S(1)} %sub.78), kind=kOutput, calls=%fused_computation.52 | convolution fusion | flops 705118208 | bytes 3684352 | tf_op jit(solution)/shard_map/hqbk,kj->hqbj/dot_general | solution.py:48
  137.5 4.3 %fusion.28 = (f32[1,256,1536]{1,2,0:T(8,128)}, f32[1,256,1536]{1,2,0:T(8,128)}) fusion(s32[256]{0:T(256)S(1)} %iota_add_fusion.2, f32[]{:T(128)} %bitcast.10, bf16[2048,128]{1,0:T(8,128)(2,1)} %copy-done.14, bf16[2048,128]{1,0:T(8,128)(2,1)S(1)} %copy-done.16), kind=kOutput, calls=%fused_computation.48 | convolution fusion | flops 104988672 | bytes 3606016 | tf_op jit(solution)/shard_map/qhd,kd->hqk/dot_general | solution.py:90
  141.9 1.5 reduce_sum.107
  143.5 3.6 %convolution_add_fusion.2 = f32[256,12,128]{0,2,1:T(8,128)} fusion(f32[256,12,128]{0,2,1:T(8,128)} %bitcast.224, f32[256,12]{0,1:T(8,128)S(1)} %sub.77), kind=kOutput, calls=%fused_computation.53 | convolution fusion | flops 604389376 | bytes 3158016 | tf_op jit(solution)/shard_map/hqbk,kj->hqbj/dot_general | solution.py:48
  147.1 4.1 %fusion.39 = (f32[1,256,1280]{1,2,0:T(8,128)}, f32[1,256,1280]{1,2,0:T(8,128)}) fusion(s32[256]{0:T(256)S(1)} %iota_add_fusion.3, f32[]{:T(128)} %bitcast.10, bf16[2048,128]{1,0:T(8,128)(2,1)} %copy-done.14, bf16[2048,128]{1,0:T(8,128)(2,1)S(1)} %copy-done.17), kind=kOutput, calls=%fused_computation.73 | convolution fusion | flops 87490560 | bytes 3016192 | tf_op jit(solution)/shard_map/qhd,kd->hqk/dot_general | solution.py:90
  151.2 1.4 reduce_sum.106
  152.6 3.2 %convolution_add_fusion.3 = f32[256,10,128]{0,2,1:T(8,128)} fusion(f32[256,10,128]{0,2,1:T(8,128)} %bitcast.226, f32[256,10]{0,1:T(8,128)S(1)} %sub.76), kind=kOutput, calls=%fused_computation.54 | convolution fusion | flops 503660544 | bytes 2631680 | tf_op jit(solution)/shard_map/hqbk,kj->hqbj/dot_general | solution.py:48
  155.9 3.7 %fusion.79 = (f32[1,256,1024]{1,2,0:T(8,128)}, f32[1,256,1024]{1,2,0:T(8,128)}) fusion(s32[256]{0:T(256)S(1)} %iota_add_fusion.4, f32[]{:T(128)} %bitcast.10, bf16[2048,128]{1,0:T(8,128)(2,1)} %copy-done.14, bf16[2048,128]{1,0:T(8,128)(2,1)S(1)} %copy-done.18), kind=kOutput, calls=%fused_computation.128 | convolution fusion | flops 69992448 | bytes 2426368 | tf_op jit(solution)/shard_map/qhd,kd->hqk/dot_general | solution.py:90
  159.6 1.3 reduce_sum.105
  160.9 3.1 %convolution_add_fusion.4 = f32[256,8,128]{0,2,1:T(8,128)} fusion(f32[256,8,128]{0,2,1:T(8,128)} %bitcast.228, f32[256,8]{0,1:T(8,128)S(1)} %sub.75), kind=kOutput, calls=%fused_computation.55 | convolution fusion | flops 402931712 | bytes 2105344 | tf_op jit(solution)/shard_map/hqbk,kj->hqbj/dot_general | solution.py:48
  164.0 3.4 %fusion.88 = (f32[1,256,768]{1,2,0:T(8,128)}, f32[1,256,768]{1,2,0:T(8,128)}) fusion(s32[256]{0:T(256)S(1)} %iota_add_fusion.5, f32[]{:T(128)} %bitcast.10, bf16[2048,128]{1,0:T(8,128)(2,1)} %copy-done.14, bf16[2048,128]{1,0:T(8,128)(2,1)} %get-tuple-element.22), kind=kOutput, calls=%fused_computation.138 | convolution fusion | flops 52494336 | bytes 1836544 | tf_op jit(solution)/shard_map/qhd,kd->hqk/dot_general | solution.py:90
  167.4 1.2 reduce_sum.104
  168.6 2.6 %convolution_add_fusion.5 = f32[256,6,128]{0,2,1:T(8,128)} fusion(f32[256,6,128]{0,2,1:T(8,128)} %bitcast.230, f32[256,6]{0,1:T(8,128)S(1)} %sub.74), kind=kOutput, calls=%fused_computation.75 | convolution fusion | flops 302202880 | bytes 1579008 | tf_op jit(solution)/shard_map/hqbk,kj->hqbj/dot_general | solution.py:48
  171.2 3.0 %fusion.99 = (f32[1,256,512]{1,2,0:T(8,128)}, f32[1,256,512]{1,2,0:T(8,128)}) fusion(s32[256]{0:T(256)S(1)} %iota_add_fusion.6, f32[]{:T(128)} %bitcast.10, bf16[2048,128]{1,0:T(8,128)(2,1)} %copy-done.14, bf16[2048,128]{1,0:T(8,128)(2,1)} %get-tuple-element.22), kind=kOutput, calls=%fused_computation.151 | convolution fusion | flops 34996224 | bytes 1246720 | tf_op jit(solution)/shard_map/qhd,kd->hqk/dot_general | solution.py:90
  174.2 1.1 reduce_sum.103
  175.3 2.2 convolution_add_fusion.6
  177.6 1.0 reduce_sum.102
  178.6 1.2 convolution_add_fusion.7
  179.9 1.1 fusion.112
  181.2 3.7 %fusion.12 = bf16[1,256,2048]{1,2,0:T(8,128)(2,1)S(1)} fusion(f32[256,16,128]{0,2,1:T(8,128)S(1)} %convolution_add_fusion, f32[1,256,2048]{1,2,0:T(8,128)} %get-tuple-element.20, s32[256]{0:T(256)S(1)} %iota_add_fusion), kind=kLoop, calls=%fused_computation.29 | loop fusion | flops 6291456 | bytes 5243904 | tf_op jit(solution)/shard_map/convert_element_type | solution.py:97
  185.0 1.5 fusion.19
  186.8 1.3 fusion.26
  188.2 0.4 copy-done.10
  188.6 1.1 fusion.37
  190.1 0.9 fusion.77
  191.1 0.7 fusion.86
  192.2 0.4 fusion.97
  194.5 0.4 fusion.49
  195.1 22.6 %all_to_all.33 = bf16[16,128,128]{1,2,0:T(8,128)(2,1)S(1)} all-to-all(bf16[16,128,128]{1,2,0:T(8,128)(2,1)S(1)} %copy.39), channel_id=1, replica_groups=mesh['sp'=16,'dp'=48] {'sp'}, dimensions={0} | all-to-all | bytes 1048576 | tf_op jit(solution)/shard_map/all_to_all | solution.py:108
  217.7 1.0 copy.40
  (93 shorter events, 5.4 us)
Async XLA Ops:
  6.5 3.6 %copy-start = (bf16[43,2048]{1,0:T(8,128)(2,1)S(1)}, bf16[43,2048]{1,0:T(8,128)(2,1)}, u32[]{:S(2)}) copy-start(bf16[43,2048]{1,0:T(8,128)(2,1)} %param.10) | copy-start | bytes 528388
  6.5 102.4 %all-gather.2.cloned.1.call-start = ((), (), s32[]{:S(2)}) async-start(), calls=%async_computation.3 | async-start | bytes 8982528 | tf_op jit(solution)/shard_map/all_gather | solution.py:76
  7.9 22.0 %copy-start.19 = (bf16[1,128,512]{2,1,0:T(8,128)(2,1)S(1)}, bf16[1,128,512]{2,1,0:T(8,128)(2,1)}, u32[]{:S(2)}) copy-start(bf16[1,128,512]{2,1,0:T(8,128)(2,1)} %param.12) | copy-start | bytes 393220
  10.1 19.9 %copy-start.20 = (bf16[1,128,512]{2,1,0:T(8,128)(2,1)S(1)}, bf16[1,128,512]{2,1,0:T(8,128)(2,1)}, u32[]{:S(2)}) copy-start(bf16[1,128,512]{2,1,0:T(8,128)(2,1)} %param.14) | copy-start | bytes 393220
  11.1 44.5 %all-to-all-start.1 = ((bf16[48,43,128]{2,1,0:T(8,128)(2,1)}), bf16[48,43,128]{2,1,0:T(8,128)(2,1)S(1)}, u32[]{:S(2)}, u32[]{:S(2)}) async-start(bf16[48,43,128]{2,1,0:T(8,128)(2,1)} %broadcast_in_dim.47), calls=%async_computation.1 | async-start | bytes 1179648 | tf_op jit(solution)/shard_map/all_to_all | solution.py:15
  30.3 37.0 %copy-start.23 = (f32[16]{0:T(128)S(1)}, f32[16]{0:T(128)}, u32[]{:S(2)}) copy-start(f32[16]{0:T(128)} %param.15) | copy-start | bytes 196
  56.9 44.1 %all-to-all-start = ((bf16[128,2,16,128]{3,0,1,2:T(8,128)(2,1)}), bf16[128,2,16,128]{3,0,1,2:T(8,128)(2,1)S(1)}, u32[]{:S(2)}, u32[]{:S(2)}) async-start(bf16[128,2,16,128]{3,0,1,2:T(8,128)(2,1)} %bitcast), calls=%async_computation | async-start | bytes 2097152 | tf_op jit(solution)/shard_map/all_to_all | solution.py:68
  101.4 13.9 %copy-start.21 = (f32[128]{0:T(128)S(1)}, f32[128]{0:T(128)}, u32[]{:S(2)}) copy-start(f32[128]{0:T(128)} %param.11) | copy-start | bytes 1540
  101.4 13.9 %copy-start.22 = (f32[128]{0:T(128)S(1)}, f32[128]{0:T(128)}, u32[]{:S(2)}) copy-start(f32[128]{0:T(128)} %param.13) | copy-start | bytes 1540
  116.7 3.7 %copy-start.14 = (bf16[2048,128]{1,0:T(8,128)(2,1)}, bf16[2048,128]{1,0:T(8,128)(2,1)S(1)}, u32[]{:S(2)}) copy-start(bf16[2048,128]{1,0:T(8,128)(2,1)S(1)} %get-tuple-element.21) | copy-start | bytes 1572868
  120.4 1.3 copy-start.1
  121.8 2.9 %copy-start.15 = (bf16[2048,128]{1,0:T(8,128)(2,1)S(1)}, bf16[2048,128]{1,0:T(8,128)(2,1)}, u32[]{:S(2)}) copy-start(bf16[2048,128]{1,0:T(8,128)(2,1)} %get-tuple-element.22) | copy-start | bytes 1572868
  133.6 3.9 %copy-start.16 = (bf16[2048,128]{1,0:T(8,128)(2,1)S(1)}, bf16[2048,128]{1,0:T(8,128)(2,1)}, u32[]{:S(2)}) copy-start(bf16[2048,128]{1,0:T(8,128)(2,1)} %get-tuple-element.22) | copy-start | bytes 1572868
  143.5 3.6 %copy-start.17 = (bf16[2048,128]{1,0:T(8,128)(2,1)S(1)}, bf16[2048,128]{1,0:T(8,128)(2,1)}, u32[]{:S(2)}) copy-start(bf16[2048,128]{1,0:T(8,128)(2,1)} %get-tuple-element.22) | copy-start | bytes 1572868
  152.6 3.3 %copy-start.18 = (bf16[2048,128]{1,0:T(8,128)(2,1)S(1)}, bf16[2048,128]{1,0:T(8,128)(2,1)}, u32[]{:S(2)}) copy-start(bf16[2048,128]{1,0:T(8,128)(2,1)} %get-tuple-element.22) | copy-start | bytes 1572868
  181.2 3.8 %copy-start.2 = (f32[256,14,128]{0,2,1:T(8,128)S(1)}, f32[256,14,128]{0,2,1:T(8,128)}, u32[]{:S(2)}) copy-start(f32[256,14,128]{0,2,1:T(8,128)} %convolution_add_fusion.1) | copy-start | bytes 5505028
  181.2 3.8 %copy-start.8 = (f32[1,256,1792]{1,2,0:T(8,128)S(1)}, f32[1,256,1792]{1,2,0:T(8,128)}, u32[]{:S(2)}) copy-start(f32[1,256,1792]{1,2,0:T(8,128)} %get-tuple-element.18) | copy-start | bytes 5505028
  185.0 1.6 copy-start.3
  185.0 1.9 copy-start.9
  186.8 1.3 copy-start.4
  186.8 1.7 copy-start.10
  188.6 1.2 copy-start.5
  188.6 1.5 copy-start.11
  189.7 1.3 copy-start.6
  189.7 1.5 copy-start.12
  191.0 1.1 copy-start.7
  191.0 1.2 copy-start.13
Sparse Core Ops, SparseCore 0:
  10.3 98.6 all-gather.1
where the time goes:
time: 227 us; the launch traced here: 226 us
  waiting for transfers between devices  65.8 us (29%)
  matrix products  60.5 us (27%)
  starting transfers between devices  29.3 us (13%)
  other arithmetic  26.4 us (12%)
  blocking collectives  22.6 us (10%)
  between operations  13.9 us (6%)
  local copies, waits for them, and re-layouts  7.16 us (3%)
    all_to_all x1, waiting for transfers between devices, body(): lax.all_to_all(copied, 'sp', split_axis=2, concat_axis=0, tiled=True)  32.8 us
    dot_general x8, matrix products, body(): jnp.einsum('qhd,kd->hqk', mine[first:finish], key_heads[:finish], preferr...  29.5 us
    all_to_all x1, waiting for transfers between devices, sent_to_all(): return lax.all_to_all(copies, axis, split_axis=0, concat_axis=0, tiled=True)  25.4 us
    dot_general x8, matrix products, stick_weights(): jnp.einsum('hqbk,kj->hqbj', pieces, upper, precision=lax.Precision.HIGHEST)  22.8 us
    all_to_all x1, blocking collectives, body(): lax.all_to_all(attended, 'sp', split_axis=0, concat_axis=1, tiled=True)  22.6 us
    all_to_all x1, starting transfers between devices, sent_to_all(): return lax.all_to_all(copies, axis, split_axis=0, concat_axis=0, tiled=True)  18.8 us
    convert_element_type x8, other arithmetic, body(): weights = stick_weights(scores, first).astype(jnp.bfloat16)  10.8 us
    all_to_all x1, starting transfers between devices, body(): lax.all_to_all(copied, 'sp', split_axis=2, concat_axis=0, tiled=True)  10.4 us
  transfers between devices with their start and end apart: 3, of which 3 were waited for; matrix products, arithmetic and copies ran while one was open for 2% of the time, Pallas kernels for 0%

commit v1 on v0

v1 whole, which is shorter than its diff:
```python
import jax
import jax.numpy as jnp
from jax import lax
from jax.experimental import pallas as pl
from jax.experimental.pallas import tpu as pltpu
from jax.sharding import Mesh, PartitionSpec as P


norm_eps = 1e-06
log2_e = 1.4426950408889634
tile = 256
low_y, cores, low_x = 2, 2, 4
group = low_y * cores


def block_step(k, v_t, q, upper, offset, carry, mask):
    scores = jnp.dot(k, q, preferred_element_type=jnp.float32) + offset
    keep = jnp.log2(1.0 + jnp.exp2(scores))
    if mask is not None:
        keep = jnp.where(mask, keep, 0.0)
    tail = jnp.dot(upper, keep.astype(jnp.bfloat16), preferred_element_type=jnp.float32)
    weights = jnp.exp2((scores - keep) - (tail + carry))
    if mask is not None:
        weights = jnp.where(mask, weights, 0.0)
    part = jnp.dot(v_t, weights.astype(jnp.bfloat16), preferred_element_type=jnp.float32)
    return part, carry + (tail[0:1] + keep[0:1])


def attend_kernel(
    place, offsets, w_own, w_left, w_right, w_low, w_high, x_own, x_core, x_far, x_both,
    kv_own, kv_one, kv_two, kv_three, gain, out, q_rows, total, carries,
):
    part, chip, core, column = place[0], place[1], place[2], place[3]
    member = chip * cores + core
    head_width = gain.shape[0]
    heads = offsets.shape[0]
    span = w_own.shape[0]
    half_span = w_low.shape[0]
    queries = None
    sources = ((w_own, 0, 0), (w_left, 3, 0), (w_right, 1, 0), (w_low, 2, 0), (w_high, 2, half_span))
    for weight, shift, begin in sources:
        start = pl.multiple_of(lax.rem(column + shift, low_x) * span + begin, 16)
        rows = pl.ds(start, weight.shape[0])
        own, near, far, both = x_own[rows], x_core[rows], x_far[rows], x_both[rows]
        flip = core == 0
        wide = jnp.concatenate(
            [
                jnp.where(flip, own, near),
                jnp.where(flip, near, own),
                jnp.where(flip, far, both),
                jnp.where(flip, both, far),
            ],
            axis=1,
        )
        term = lax.dot_general(
            weight[...], wide, (((0,), (0,)), ((), ())), preferred_element_type=jnp.float32
        )
        queries = term if queries is None else queries + term
    for h in range(heads):
        for t in range(2):
            rows = queries[h * head_width : (h + 1) * head_width, t * tile : (t + 1) * tile]
            rows = rows.astype(jnp.bfloat16).astype(jnp.float32)
            mean = jnp.mean(rows * rows, axis=0, keepdims=True)
            scaled = rows * lax.rsqrt(mean + norm_eps) * gain[:, 0:1]
            q_rows[jnp.bitwise_xor(chip, t), h] = scaled.astype(jnp.bfloat16)
    row_id = lax.broadcasted_iota(jnp.int32, (tile, tile), 0)
    column_id = lax.broadcasted_iota(jnp.int32, (tile, tile), 1)
    upper = (column_id > row_id).astype(jnp.float32).astype(jnp.bfloat16)
    mask = row_id < column_id

    def block_of(kv, index):
        left = kv[jnp.bitwise_xor(2 * index, member)]
        right = kv[jnp.bitwise_xor(2 * index + 1, member)]
        k = jnp.concatenate([left[0], right[0]], axis=0)
        return k, jnp.concatenate([left[1], right[1]], axis=1)

    zero = jnp.zeros((1, tile), jnp.float32)
    first, last = block_of(kv_own, 0), block_of(kv_own, 1)
    for h in range(heads):
        offset = offsets[h]
        piece, carry = block_step(*last, q_rows[1, h], upper, offset, zero, mask)
        more, carry = block_step(*first, q_rows[1, h], upper, offset, carry, None)
        total[h, 1] = piece + more
        carries[h, 1] = jnp.broadcast_to(carry, (8, tile))
        piece, carry = block_step(*first, q_rows[0, h], upper, offset, zero, mask)
        total[h, 0] = piece
        carries[h, 0] = jnp.broadcast_to(carry, (8, tile))

    for distance, kv in ((1, kv_one), (2, kv_two), (3, kv_three)):

        @pl.when(part >= distance)
        def _(kv=kv):
            blocks = (block_of(kv, 1), block_of(kv, 0))
            for h in range(heads):
                for t in range(2):
                    carry, summed = carries[h, t, 0:1], total[h, t]
                    for k, v_t in blocks:
                        piece, carry = block_step(
                            k, v_t, q_rows[t, h], upper, offsets[h], carry, None
                        )
                        summed = summed + piece
                    total[h, t] = summed
                    carries[h, t] = jnp.broadcast_to(carry, (8, tile))

    half = tile // 2
    for h in range(heads):
        for t in range(2):
            rows = total[h, t].T.astype(jnp.bfloat16)
            for c in range(2):
                out[2 * t + c, :, h * head_width : (h + 1) * head_width] = rows[
                    c * half : (c + 1) * half
                ]


def attend(place, offsets, weights, xs, kvs, gain):
    heads = offsets.shape[0]
    head_width = gain.shape[0]
    vmem = pl.BlockSpec(memory_space=pltpu.VMEM)
    smem = pl.BlockSpec(memory_space=pltpu.SMEM)
    flops = 2 * xs[0].size * heads * head_width * group
    flops += heads * 8 * 2 * tile * tile * (2 * head_width + tile)
    return pl.pallas_call(
        attend_kernel,
        out_shape=jax.ShapeDtypeStruct((group, tile // 2, heads * head_width), jnp.bfloat16),
        in_specs=[smem, smem, *[vmem] * 14],
        out_specs=vmem,
        scratch_shapes=[
            pltpu.VMEM((2, heads, head_width, tile), jnp.bfloat16),
            pltpu.VMEM((heads, 2, head_width, tile), jnp.float32),
            pltpu.VMEM((heads, 2, 8, tile), jnp.float32),
        ],
        cost_estimate=pl.CostEstimate(flops=flops, bytes_accessed=1 << 22, transcendentals=0),
    )(place, offsets, *weights, *xs, *kvs, gain)


def sent_to_all(value, axes):
    count = lax.axis_size(axes)
    copies = jnp.broadcast_to(value, (count, *value.shape))
    return lax.all_to_all(copies, axes, split_axis=0, concat_axis=0, tiled=True)


def swapped(value, axis):
    return lax.ppermute(value, axis, [(0, 1), (1, 0)])


def turned(value, axis, shift):
    count = lax.axis_size(axis)
    return lax.ppermute(value, axis, [(i, (i + shift) % count) for i in range(count)])


def flipped(value, bits):
    return lax.ppermute(value, ("yl", "core"), [(i, i ^ bits) for i in range(group)])


def handed_on(value, shift):
    count = lax.axis_size("yh")
    return lax.ppermute(value, "yh", [(i, i + shift) for i in range(count - shift)])


def layer(stream, mix_gain, query_weight, query_gain, keys, key_gain, values, stick_offset):
    part, chip, core = lax.axis_index("yh"), lax.axis_index("yl"), lax.axis_index("core")
    member = chip * cores + core
    head_width = query_gain.shape[0]
    heads_all = stick_offset.shape[0]
    heads = heads_all // group
    rows_dev = query_weight.shape[0]
    padded = -(-rows_dev // 16) * 16
    span = heads * head_width
    tokens = stream.shape[1]

    columns = lax.dynamic_slice_in_dim(query_weight, member * span, span, 1)
    columns = jnp.pad(columns, ((0, padded - rows_dev), (0, 0)))
    along_z = sent_to_all(columns, "z").reshape(-1, span)

    kv_heads = keys.shape[2] // head_width
    k = keys[0].reshape(tokens, kv_heads, head_width).astype(jnp.float32)
    k = k * lax.rsqrt(jnp.mean(k * k, axis=-1, keepdims=True) + norm_eps) * key_gain
    k = k.astype(jnp.bfloat16).transpose(1, 0, 2)
    v = values[0].reshape(tokens, kv_heads, head_width).transpose(1, 2, 0)
    kv = jnp.stack((k, v), axis=1)
    pieces = [lax.dynamic_index_in_dim(kv, member ^ bits, 0, keepdims=True) for bits in range(group)]
    pieces[1:] = [flipped(pieces[bits], bits) for bits in range(1, group)]
    kv_own = jnp.concatenate(pieces, axis=0)
    kvs = (kv_own, *[handed_on(kv_own, shift) for shift in range(1, lax.axis_size("yh"))])

    x_t = stream[0].T.astype(jnp.float32)
    scale = lax.rsqrt(jnp.mean(x_t * x_t, axis=0, keepdims=True) + norm_eps)
    normed = (x_t * scale * mix_gain[:, None]).astype(jnp.bfloat16)
    normed = normed.reshape(-1, low_x, rows_dev, tokens).transpose(1, 0, 2, 3)
    normed = jnp.pad(normed, ((0, 0), (0, 0), (0, padded - rows_dev), (0, 0)))
    normed = normed.reshape(-1, tokens)
    far = swapped(normed, "yl")
    near = swapped(normed, "core")
    xs = (normed, near, far, swapped(far, "core"))

    left, right = turned(along_z, "x", 1), turned(along_z, "x", -1)
    half = along_z.shape[0] // 2
    low, high = turned(left[:half], "x", 1), turned(right[half:], "x", -1)
    weights = (along_z, left, right, low, high)

    gain = query_gain * (head_width ** (-0.5) * log2_e)
    gain = jnp.broadcast_to(gain[:, None], (head_width, head_width))
    place = jnp.stack((part, chip, core, lax.axis_index("x"))).astype(jnp.int32)
    offsets = lax.dynamic_slice_in_dim(stick_offset * log2_e, member * heads, heads)
    attended = attend(place, offsets, weights, xs, kvs, gain)
    out = lax.all_to_all(attended, ("yl", "core"), split_axis=0, concat_axis=0, tiled=True)
    return out.transpose(1, 0, 2).reshape(1, tokens, heads_all * head_width)


def solution(mesh):
    sp, dp = mesh.shape["sp"], mesh.shape["dp"]
    fine = Mesh(
        mesh.devices.reshape(sp // group, low_y, cores, dp // low_x, low_x),
        ("yh", "yl", "core", "z", "x"),
    )
    along, across = ("yh", "yl", "core"), ("z", "x")
    return jax.shard_map(
        layer,
        mesh=fine,
        in_specs=(
            P(across, along, None),
            P(),
            P(across, None),
            P(),
            P(across, along, None),
            P(),
            P(across, along, None),
            P(),
        ),
        out_specs=P(across, along, None),
        check_vma=False,
    )
```

time: 227 us -> 146 us (0.64)
  the two profiles are of different devices: /device:TPU:1 before, /device:TPU:112 now
where the time goes in v1:
time: 146 us; the launch traced here: 145 us
  waiting for transfers between devices  54.1 us (37%)
  starting transfers between devices  47.1 us (32%)
  Pallas kernels  24.3 us (17%)
  blocking collectives  12.3 us (8%)
  local copies, waits for them, and re-layouts  5.19 us (4%)
  other arithmetic  1.49 us (1%)
    pallas_call x1, Pallas kernels, attend(): pl.pallas_call(attend_kernel, out_shape=jax.ShapeDtypeStruct((group, tile...  24.3 us
    all_to_all x1, waiting for transfers between devices, sent_to_all(): return lax.all_to_all(copies, axes, split_axis=0, concat_axis=0, tiled=True)  22 us
    ppermute x3, waiting for transfers between devices, handed_on(): lax.ppermute(value, 'yh', [(i, i + shift) for i in range(count - shift)])  21.1 us
    all_to_all x1, starting transfers between devices, sent_to_all(): return lax.all_to_all(copies, axes, split_axis=0, concat_axis=0, tiled=True)  14.9 us
    ppermute x4, starting transfers between devices, turned(): lax.ppermute(value, axis, [(i, (i + shift) % count) for i in range(count)])  13.6 us
    all_to_all x1, blocking collectives, layer(): lax.all_to_all(attended, ('yl', 'core'), split_axis=0, concat_axis=0, til...  12.3 us
    ppermute x4, waiting for transfers between devices, turned(): lax.ppermute(value, axis, [(i, (i + shift) % count) for i in range(count)])  8.22 us
    ppermute x3, starting transfers between devices, flipped(): lax.ppermute(value, ('yl', 'core'), [(i, i ^ bits) for i in range(group)])  7.59 us
  transfers between devices with their start and end apart: 14, of which 6 were waited for; matrix products, arithmetic and copies ran while one was open for 2% of the time, Pallas kernels for 0%

profile of v1, /device:TPU:112, one launch (start us, length us, event | category | flops | bytes accessed | tf_op | source)
XLA Modules:
  0.0 144.9 jit_solution(3581669835977086921)
XLA Ops:
  0.0 0.9 copy-done
  0.9 0.9 broadcast_in_dim.4
  1.8 14.9 %all-to-all-start = ((bf16[12,48,512]{2,1,0:T(8,128)(2,1)}), bf16[12,48,512]{2,1,0:T(8,128)(2,1)S(1)}, u32[]{:S(2)}, u32[]{:S(2)}) async-start(bf16[12,48,512]{2,1,0:T(8,128)(2,1)} %broadcast_in_dim.4), calls=%async_computation | async-start | bytes 1179648 | tf_op jit(solution)/shard_map/all_to_all | solution.py:139
  16.7 0.3 fusion
  17.0 0.3 fusion.3
  17.4 0.2 reshape.36
  17.6 0.0 copy-start.7
  17.6 0.1 pad.9.clone
  17.7 0.0 copy-start.8
  17.7 0.0 copy-start.10
  17.7 2.7 %collective-permute-start.5 = (bf16[2304,128]{1,0:T(8,128)(2,1)S(1)}, bf16[2304,128]{1,0:T(8,128)(2,1)}, u32[]{:S(2)}, u32[]{:S(2)}) collective-permute-start(bf16[2304,128]{1,0:T(8,128)(2,1)S(1)} %bitcast.34), channel_id=1, source_target_pairs={{0,96},{96,0},{1,97},{97,1},{2,98},{98,2},{3,99},{99,3},{4,100},{1... | collective-permute-start | bytes 1769480 | tf_op jit(solution)/shard_map/ppermute | solution.py:143
  20.5 0.1 copy.12
  20.6 0.1 copy.13
  20.7 0.1 copy.14
  20.9 22.0 %all-to-all-done = bf16[12,48,512]{2,1,0:T(8,128)(2,1)S(1)} async-done(((bf16[12,48,512]{2,1,0:T(8,128)(2,1)}), bf16[12,48,512]{2,1,0:T(8,128)(2,1)S(1)}, u32[]{:S(2)}, u32[]{:S(2)}) %all-to-all-start) | async-done | bytes 589856 | tf_op jit(solution)/shard_map/all_to_all | solution.py:139
  42.9 4.7 %collective-permute-start.1 = (bf16[576,512]{1,0:T(8,128)(2,1)S(1)}, bf16[576,512]{1,0:T(8,128)(2,1)S(1)}, u32[]{:S(2)}, u32[]{:S(2)}) collective-permute-start(bf16[576,512]{1,0:T(8,128)(2,1)S(1)} %bitcast.31), channel_id=1, source_target_pairs={{0,3},{1,0},{2,1},{3,2},{4,7},{5,4},{6,5},{7,6},{8,11},{9,8},{10,9... | collective-permute-start | bytes 1769480 | tf_op jit(solution)/shard_map/ppermute | solution.py:148
  47.6 0.1 fusion.4
  47.7 0.0 copy-start.15
  47.7 1.9 %collective-permute-start = (bf16[576,512]{1,0:T(8,128)(2,1)S(1)}, bf16[576,512]{1,0:T(8,128)(2,1)S(1)}, u32[]{:S(2)}, u32[]{:S(2)}) collective-permute-start(bf16[576,512]{1,0:T(8,128)(2,1)S(1)} %bitcast.32), channel_id=1, source_target_pairs={{0,1},{1,2},{2,3},{3,0},{4,5},{5,6},{6,7},{7,4},{8,9},{9,10},{10,1... | collective-permute-start | bytes 1769480 | tf_op jit(solution)/shard_map/ppermute | solution.py:148
  49.7 1.9 %collective-permute-start.7 = (bf16[1,2,128,128]{3,2,1,0:T(8,128)(2,1)S(1)}, bf16[1,2,128,128]{3,2,1,0:T(8,128)(2,1)S(1)}, u32[]{:S(2)}, u32[]{:S(2)}) collective-permute-start(bf16[1,2,128,128]{3,2,1,0:T(8,128)(2,1)S(1)} %get-tuple-element.6), channel_id=1, source_target_pairs={{0,48},{48,0},{96,144},{144,96},{1,49},{49,1},{97,145},{145,97},{2... | collective-permute-start | bytes 196616 | tf_op jit(solution)/shard_map/ppermute | solution.py:152
  51.6 2.6 %collective-permute-start.8 = (bf16[1,2,128,128]{3,2,1,0:T(8,128)(2,1)S(1)}, bf16[1,2,128,128]{3,2,1,0:T(8,128)(2,1)S(1)}, u32[]{:S(2)}, u32[]{:S(2)}) collective-permute-start(bf16[1,2,128,128]{3,2,1,0:T(8,128)(2,1)S(1)} %get-tuple-element.7), channel_id=1, source_target_pairs={{0,96},{48,144},{96,0},{144,48},{1,97},{49,145},{97,1},{145,49},{2... | collective-permute-start | bytes 196616 | tf_op jit(solution)/shard_map/ppermute | solution.py:152
  54.2 0.0 collective-permute-done.7
  54.2 3.1 %collective-permute-start.9 = (bf16[1,2,128,128]{3,2,1,0:T(8,128)(2,1)S(1)}, bf16[1,2,128,128]{3,2,1,0:T(8,128)(2,1)S(1)}, u32[]{:S(2)}, u32[]{:S(2)}) collective-permute-start(bf16[1,2,128,128]{3,2,1,0:T(8,128)(2,1)S(1)} %get-tuple-element.8), channel_id=1, source_target_pairs={{0,144},{48,96},{96,48},{144,0},{1,145},{49,97},{97,49},{145,1},{2... | collective-permute-start | bytes 196616 | tf_op jit(solution)/shard_map/ppermute | solution.py:152
  57.3 0.7 collective-permute-done.8
  58.0 2.1 %collective-permute-done.9 = bf16[1,2,128,128]{3,2,1,0:T(8,128)(2,1)S(1)} collective-permute-done((bf16[1,2,128,128]{3,2,1,0:T(8,128)(2,1)S(1)}, bf16[1,2,128,128]{3,2,1,0:T(8,128)(2,1)S(1)}, u32[]{:S(2)}, u32[]{:S(2)}) %collective-permute-start.9) | collective-permute-done | bytes 65568 | tf_op jit(solution)/shard_map/ppermute | solution.py:152
  60.2 1.3 collective-permute-start.12
  61.5 1.3 collective-permute-start.11
  62.8 0.0 collective-permute-done.5.x_far
  62.8 2.4 %collective-permute-start.4 = (bf16[2304,128]{1,0:T(8,128)(2,1)S(1)}, bf16[2304,128]{1,0:T(8,128)(2,1)}, u32[]{:S(2)}, u32[]{:S(2)}) collective-permute-start(bf16[2304,128]{1,0:T(8,128)(2,1)S(1)} %bitcast.35), channel_id=1, source_target_pairs={{0,48},{48,0},{1,49},{49,1},{2,50},{50,2},{3,51},{51,3},{4,52},{52... | collective-permute-start | bytes 1769480 | tf_op jit(solution)/shard_map/ppermute | solution.py:143
  65.2 0.0 collective-permute-done.1.w_right
  65.2 1.9 %collective-permute-start.6 = (bf16[2304,128]{1,0:T(8,128)(2,1)}, bf16[2304,128]{1,0:T(8,128)(2,1)}, u32[]{:S(2)}, u32[]{:S(2)}) collective-permute-start(bf16[2304,128]{1,0:T(8,128)(2,1)} %collective-permute-done.5.x_far), channel_id=1, source_target_pairs={{0,48},{48,0},{1,49},{49,1},{2,50},{50,2},{3,51},{51,3},{4,52},{52... | collective-permute-start | bytes 1769480 | tf_op jit(solution)/shard_map/ppermute | solution.py:143
  67.2 0.0 copy-start.16
  67.2 0.0 collective-permute-done.w_left
  67.3 1.3 collective-permute-start.10
  68.6 21.1 %collective-permute-done.12.kv_three = bf16[4,2,128,128]{3,2,1,0:T(8,128)(2,1)S(1)} collective-permute-done((bf16[4,2,128,128]{3,2,1,0:T(8,128)(2,1)S(1)}, bf16[4,2,128,128]{3,2,1,0:T(8,128)(2,1)S(1)}, u32[]{:S(2)}, u32[]{:S(2)}) %collective-permute-start.12) | collective-permute-done | bytes 262176 | tf_op jit(solution)/shard_map/ppermute | solution.py:157
  89.8 5.1 %collective-permute-start.3 = (bf16[288,512]{1,0:T(8,128)(2,1)S(1)}, bf16[288,512]{1,0:T(8,128)(2,1)S(1)}, u32[]{:S(2)}, u32[]{:S(2)}) collective-permute-start(bf16[288,512]{1,0:T(8,128)(2,1)S(1)} %slice.9), channel_id=1, source_target_pairs={{0,3},{1,0},{2,1},{3,2},{4,7},{5,4},{6,5},{7,6},{8,11},{9,8},{10,9... | collective-permute-start | bytes 884744 | tf_op jit(solution)/shard_map/ppermute | solution.py:148
  94.9 0.0 collective-permute-done.11.kv_two
  94.9 1.9 %collective-permute-start.2 = (bf16[288,512]{1,0:T(8,128)(2,1)S(1)}, bf16[288,512]{1,0:T(8,128)(2,1)S(1)}, u32[]{:S(2)}, u32[]{:S(2)}) collective-permute-start(bf16[288,512]{1,0:T(8,128)(2,1)S(1)} %slice.8), channel_id=1, source_target_pairs={{0,1},{1,2},{2,3},{3,0},{4,5},{5,6},{6,7},{7,4},{8,9},{9,10},{10,1... | collective-permute-start | bytes 884744 | tf_op jit(solution)/shard_map/ppermute | solution.py:148
  96.8 0.6 pad_add_fusion.place
  97.4 0.6 dynamic_slice.19.offsets
  98.1 0.0 collective-permute-done.6.x_both
  98.1 2.9 %collective-permute-done.3.w_high = bf16[288,512]{1,0:T(8,128)(2,1)S(1)} collective-permute-done((bf16[288,512]{1,0:T(8,128)(2,1)S(1)}, bf16[288,512]{1,0:T(8,128)(2,1)S(1)}, u32[]{:S(2)}, u32[]{:S(2)}) %collective-permute-start.3) | collective-permute-done | bytes 294944 | tf_op jit(solution)/shard_map/ppermute | solution.py:148
  101.0 5.3 %collective-permute-done.2.w_low = bf16[288,512]{1,0:T(8,128)(2,1)S(1)} collective-permute-done((bf16[288,512]{1,0:T(8,128)(2,1)S(1)}, bf16[288,512]{1,0:T(8,128)(2,1)S(1)}, u32[]{:S(2)}, u32[]{:S(2)}) %collective-permute-start.2) | collective-permute-done | bytes 294944 | tf_op jit(solution)/shard_map/ppermute | solution.py:148
  106.3 0.7 broadcast_in_dim.5.gain
  107.1 24.3 %shard_map.82 = bf16[4,128,512]{2,1,0:T(8,128)(2,1)} custom-call(s32[4]{0:T(128)} %pad_add_fusion.place, f32[4]{0:T(128)} %dynamic_slice.19.offsets, bf16[576,512]{1,0:T(8,128)(2,1)} %bitcast.33, bf16[576,512]{1,0:T(8,128)(2,1)} %copy-done.6, bf16[576,512]{1,0:T(8,128)(2,1)} %copy-done.5, bf16[288,512]{1,0:T(8,128)(2,1)} %copy-done.12, ...), custom_call_target="tpu_custom_call" | custom-call | flops 3355443200 | bytes 4194304 | tf_op jit(solution)/shard_map/pallas_call | solution.py:122
  131.4 12.3 %all_to_all.10 = bf16[4,128,512]{2,1,0:T(8,128)(2,1)S(1)} all-to-all(bf16[4,128,512]{2,1,0:T(8,128)(2,1)} %shard_map.82), channel_id=1, replica_groups=mesh['yh'=4,'yl'=2,'core'=2,'z'=12,'x'=4] {'yl','core'}, dimensions={0} | all-to-all | bytes 1048576 | tf_op jit(solution)/shard_map/all_to_all | solution.py:206
  143.6 0.3 copy.15
  143.9 1.0 copy.16
  (42 shorter events, 0.3 us)
Async XLA Ops:
  0.0 0.9 copy-start
  1.8 14.9 %copy-start.1 = (bf16[1,128,2064]{1,2,0:T(8,128)(2,1)S(1)}, bf16[1,128,2064]{1,2,0:T(8,128)(2,1)}, u32[]{:S(2)}) copy-start(bf16[1,128,2064]{1,2,0:T(8,128)(2,1)} %param.8) | copy-start | bytes 1585156
  1.8 15.2 %copy-start.9 = (f32[2064]{0:T(1024)S(1)}, f32[2064]{0:T(1024)}, u32[]{:S(2)}) copy-start(f32[2064]{0:T(1024)} %param.9) | copy-start | bytes 24772
  1.8 41.1 %all-to-all-start = ((bf16[12,48,512]{2,1,0:T(8,128)(2,1)}), bf16[12,48,512]{2,1,0:T(8,128)(2,1)S(1)}, u32[]{:S(2)}, u32[]{:S(2)}) async-start(bf16[12,48,512]{2,1,0:T(8,128)(2,1)} %broadcast_in_dim.4), calls=%async_computation | async-start | bytes 1179648 | tf_op jit(solution)/shard_map/all_to_all | solution.py:139
  17.6 2.9 %copy-start.7 = (bf16[1,128,512]{2,1,0:T(8,128)(2,1)S(1)}, bf16[1,128,512]{2,1,0:T(8,128)(2,1)}, u32[]{:S(2)}) copy-start(bf16[1,128,512]{2,1,0:T(8,128)(2,1)} %param.12) | copy-start | bytes 393220
  17.7 45.1 %copy-start.3 = (bf16[4,12,48,128]{3,2,1,0:T(8,128)(2,1)}, bf16[4,12,48,128]{3,2,1,0:T(8,128)(2,1)S(1)}, u32[]{:S(2)}) copy-start(bf16[4,12,48,128]{3,2,1,0:T(8,128)(2,1)S(1)} %pad.9.clone) | copy-start | bytes 1769476
  17.7 3.0 %copy-start.8 = (bf16[1,128,512]{2,1,0:T(8,128)(2,1)S(1)}, bf16[1,128,512]{2,1,0:T(8,128)(2,1)}, u32[]{:S(2)}) copy-start(bf16[1,128,512]{2,1,0:T(8,128)(2,1)} %param.14) | copy-start | bytes 393220
  17.7 29.8 %copy-start.10 = (f32[128]{0:T(128)S(1)}, f32[128]{0:T(128)}, u32[]{:S(2)}) copy-start(f32[128]{0:T(128)} %param.13) | copy-start | bytes 1540
  17.7 45.0 %collective-permute-start.5 = (bf16[2304,128]{1,0:T(8,128)(2,1)S(1)}, bf16[2304,128]{1,0:T(8,128)(2,1)}, u32[]{:S(2)}, u32[]{:S(2)}) collective-permute-start(bf16[2304,128]{1,0:T(8,128)(2,1)S(1)} %bitcast.34), channel_id=1, source_target_pairs={{0,96},{96,0},{1,97},{97,1},{2,98},{98,2},{3,99},{99,3},{4,100},{1... | collective-permute-start | bytes 1769480 | tf_op jit(solution)/shard_map/ppermute | solution.py:143
  42.9 17.3 %copy-start.2 = (bf16[12,48,512]{2,1,0:T(8,128)(2,1)}, bf16[12,48,512]{2,1,0:T(8,128)(2,1)S(1)}, u32[]{:S(2)}) copy-start(bf16[12,48,512]{2,1,0:T(8,128)(2,1)S(1)} %all-to-all-done) | copy-start | bytes 1769476
  42.9 22.3 %collective-permute-start.1 = (bf16[576,512]{1,0:T(8,128)(2,1)S(1)}, bf16[576,512]{1,0:T(8,128)(2,1)S(1)}, u32[]{:S(2)}, u32[]{:S(2)}) collective-permute-start(bf16[576,512]{1,0:T(8,128)(2,1)S(1)} %bitcast.31), channel_id=1, source_target_pairs={{0,3},{1,0},{2,1},{3,2},{4,7},{5,4},{6,5},{7,6},{8,11},{9,8},{10,9... | collective-permute-start | bytes 1769480 | tf_op jit(solution)/shard_map/ppermute | solution.py:148
  47.7 19.5 %copy-start.15 = (f32[16]{0:T(128)S(1)}, f32[16]{0:T(128)}, u32[]{:S(2)}) copy-start(f32[16]{0:T(128)} %param.15) | copy-start | bytes 196
  47.7 19.5 %collective-permute-start = (bf16[576,512]{1,0:T(8,128)(2,1)S(1)}, bf16[576,512]{1,0:T(8,128)(2,1)S(1)}, u32[]{:S(2)}, u32[]{:S(2)}) collective-permute-start(bf16[576,512]{1,0:T(8,128)(2,1)S(1)} %bitcast.32), channel_id=1, source_target_pairs={{0,1},{1,2},{2,3},{3,0},{4,5},{5,6},{6,7},{7,4},{8,9},{9,10},{10,1... | collective-permute-start | bytes 1769480 | tf_op jit(solution)/shard_map/ppermute | solution.py:148
  49.7 4.5 %collective-permute-start.7 = (bf16[1,2,128,128]{3,2,1,0:T(8,128)(2,1)S(1)}, bf16[1,2,128,128]{3,2,1,0:T(8,128)(2,1)S(1)}, u32[]{:S(2)}, u32[]{:S(2)}) collective-permute-start(bf16[1,2,128,128]{3,2,1,0:T(8,128)(2,1)S(1)} %get-tuple-element.6), channel_id=1, source_target_pairs={{0,48},{48,0},{96,144},{144,96},{1,49},{49,1},{97,145},{145,97},{2... | collective-permute-start | bytes 196616 | tf_op jit(solution)/shard_map/ppermute | solution.py:152
  51.6 6.4 %collective-permute-start.8 = (bf16[1,2,128,128]{3,2,1,0:T(8,128)(2,1)S(1)}, bf16[1,2,128,128]{3,2,1,0:T(8,128)(2,1)S(1)}, u32[]{:S(2)}, u32[]{:S(2)}) collective-permute-start(bf16[1,2,128,128]{3,2,1,0:T(8,128)(2,1)S(1)} %get-tuple-element.7), channel_id=1, source_target_pairs={{0,96},{48,144},{96,0},{144,48},{1,97},{49,145},{97,1},{145,49},{2... | collective-permute-start | bytes 196616 | tf_op jit(solution)/shard_map/ppermute | solution.py:152
  54.2 5.9 %collective-permute-start.9 = (bf16[1,2,128,128]{3,2,1,0:T(8,128)(2,1)S(1)}, bf16[1,2,128,128]{3,2,1,0:T(8,128)(2,1)S(1)}, u32[]{:S(2)}, u32[]{:S(2)}) collective-permute-start(bf16[1,2,128,128]{3,2,1,0:T(8,128)(2,1)S(1)} %get-tuple-element.8), channel_id=1, source_target_pairs={{0,144},{48,96},{96,48},{144,0},{1,145},{49,97},{97,49},{145,1},{2... | collective-permute-start | bytes 196616 | tf_op jit(solution)/shard_map/ppermute | solution.py:152
  60.2 8.4 %copy-start.4 = (bf16[4,2,128,128]{3,2,1,0:T(8,128)(2,1)}, bf16[4,2,128,128]{3,2,1,0:T(8,128)(2,1)S(1)}, u32[]{:S(2)}) copy-start(bf16[4,2,128,128]{3,2,1,0:T(8,128)(2,1)S(1)} %pad_maximum_fusion.kv_own) | copy-start | bytes 786436
  60.2 29.6 %collective-permute-start.12 = (bf16[4,2,128,128]{3,2,1,0:T(8,128)(2,1)S(1)}, bf16[4,2,128,128]{3,2,1,0:T(8,128)(2,1)S(1)}, u32[]{:S(2)}, u32[]{:S(2)}) collective-permute-start(bf16[4,2,128,128]{3,2,1,0:T(8,128)(2,1)S(1)} %pad_maximum_fusion.kv_own), channel_id=1, source_target_pairs={{0,576},{1,577},{2,578},{3,579},{4,580},{5,581},{6,582},{7,583},{8... | collective-permute-start | bytes 786440 | tf_op jit(solution)/shard_map/ppermute | solution.py:157
  61.5 33.4 %collective-permute-start.11 = (bf16[4,2,128,128]{3,2,1,0:T(8,128)(2,1)S(1)}, bf16[4,2,128,128]{3,2,1,0:T(8,128)(2,1)}, u32[]{:S(2)}, u32[]{:S(2)}) collective-permute-start(bf16[4,2,128,128]{3,2,1,0:T(8,128)(2,1)S(1)} %pad_maximum_fusion.kv_own), channel_id=1, source_target_pairs={{0,384},{192,576},{1,385},{193,577},{2,386},{194,578},{3,387},{195... | collective-permute-start | bytes 786440 | tf_op jit(solution)/shard_map/ppermute | solution.py:157
  62.8 35.3 %collective-permute-start.4 = (bf16[2304,128]{1,0:T(8,128)(2,1)S(1)}, bf16[2304,128]{1,0:T(8,128)(2,1)}, u32[]{:S(2)}, u32[]{:S(2)}) collective-permute-start(bf16[2304,128]{1,0:T(8,128)(2,1)S(1)} %bitcast.35), channel_id=1, source_target_pairs={{0,48},{48,0},{1,49},{49,1},{2,50},{50,2},{3,51},{51,3},{4,52},{52... | collective-permute-start | bytes 1769480 | tf_op jit(solution)/shard_map/ppermute | solution.py:143
  65.2 3.4 %copy-start.5 = (bf16[576,512]{1,0:T(8,128)(2,1)}, bf16[576,512]{1,0:T(8,128)(2,1)S(1)}, u32[]{:S(2)}) copy-start(bf16[576,512]{1,0:T(8,128)(2,1)S(1)} %collective-permute-done.1.w_right) | copy-start | bytes 1769476
  65.2 32.8 %collective-permute-start.6 = (bf16[2304,128]{1,0:T(8,128)(2,1)}, bf16[2304,128]{1,0:T(8,128)(2,1)}, u32[]{:S(2)}, u32[]{:S(2)}) collective-permute-start(bf16[2304,128]{1,0:T(8,128)(2,1)} %collective-permute-done.5.x_far), channel_id=1, source_target_pairs={{0,48},{48,0},{1,49},{49,1},{2,50},{50,2},{3,51},{51,3},{4,52},{52... | collective-permute-start | bytes 1769480 | tf_op jit(solution)/shard_map/ppermute | solution.py:143
  67.2 30.8 %copy-start.16 = (f32[128]{0:T(128)S(1)}, f32[128]{0:T(128)}, u32[]{:S(2)}) copy-start(f32[128]{0:T(128)} %param.11) | copy-start | bytes 1540
  67.3 39.8 %copy-start.6 = (bf16[576,512]{1,0:T(8,128)(2,1)}, bf16[576,512]{1,0:T(8,128)(2,1)S(1)}, u32[]{:S(2)}) copy-start(bf16[576,512]{1,0:T(8,128)(2,1)S(1)} %collective-permute-done.w_left) | copy-start | bytes 1769476
  67.3 30.8 %collective-permute-start.10 = (bf16[4,2,128,128]{3,2,1,0:T(8,128)(2,1)S(1)}, bf16[4,2,128,128]{3,2,1,0:T(8,128)(2,1)S(1)}, u32[]{:S(2)}, u32[]{:S(2)}) collective-permute-start(bf16[4,2,128,128]{3,2,1,0:T(8,128)(2,1)S(1)} %pad_maximum_fusion.kv_own), channel_id=1, source_target_pairs={{0,192},{192,384},{384,576},{1,193},{193,385},{385,577},{2,194},{1... | collective-permute-start | bytes 786440 | tf_op jit(solution)/shard_map/ppermute | solution.py:157
  89.8 17.3 %copy-start.13 = (bf16[4,2,128,128]{3,2,1,0:T(8,128)(2,1)}, bf16[4,2,128,128]{3,2,1,0:T(8,128)(2,1)S(1)}, u32[]{:S(2)}) copy-start(bf16[4,2,128,128]{3,2,1,0:T(8,128)(2,1)S(1)} %collective-permute-done.12.kv_three) | copy-start | bytes 786436
  89.8 11.2 %collective-permute-start.3 = (bf16[288,512]{1,0:T(8,128)(2,1)S(1)}, bf16[288,512]{1,0:T(8,128)(2,1)S(1)}, u32[]{:S(2)}, u32[]{:S(2)}) collective-permute-start(bf16[288,512]{1,0:T(8,128)(2,1)S(1)} %slice.9), channel_id=1, source_target_pairs={{0,3},{1,0},{2,1},{3,2},{4,7},{5,4},{6,5},{7,6},{8,11},{9,8},{10,9... | collective-permute-start | bytes 884744 | tf_op jit(solution)/shard_map/ppermute | solution.py:148
  94.9 11.4 %collective-permute-start.2 = (bf16[288,512]{1,0:T(8,128)(2,1)S(1)}, bf16[288,512]{1,0:T(8,128)(2,1)S(1)}, u32[]{:S(2)}, u32[]{:S(2)}) collective-permute-start(bf16[288,512]{1,0:T(8,128)(2,1)S(1)} %slice.8), channel_id=1, source_target_pairs={{0,1},{1,2},{2,3},{3,0},{4,5},{5,6},{6,7},{7,4},{8,9},{9,10},{10,1... | collective-permute-start | bytes 884744 | tf_op jit(solution)/shard_map/ppermute | solution.py:148
  98.0 9.0 %copy-start.14 = (bf16[4,2,128,128]{3,2,1,0:T(8,128)(2,1)}, bf16[4,2,128,128]{3,2,1,0:T(8,128)(2,1)S(1)}, u32[]{:S(2)}) copy-start(bf16[4,2,128,128]{3,2,1,0:T(8,128)(2,1)S(1)} %collective-permute-done.10.kv_one) | copy-start | bytes 786436
  101.0 6.1 %copy-start.11 = (bf16[288,512]{1,0:T(8,128)(2,1)}, bf16[288,512]{1,0:T(8,128)(2,1)S(1)}, u32[]{:S(2)}) copy-start(bf16[288,512]{1,0:T(8,128)(2,1)S(1)} %collective-permute-done.3.w_high) | copy-start | bytes 884740
  106.3 0.8 copy-start.12

commit v2 on v1

--- a/solution.py
+++ b/solution.py
@@ -9,25 +9,44 @@
 norm_eps = 1e-06
 log2_e = 1.4426950408889634
 tile = 256
+sublanes = 8
 low_y, cores, low_x = 2, 2, 4
 group = low_y * cores
 
 
-def block_step(k, v_t, q, upper, offset, carry, mask):
-    scores = jnp.dot(k, q, preferred_element_type=jnp.float32) + offset
-    keep = jnp.log2(1.0 + jnp.exp2(scores))
-    if mask is not None:
-        keep = jnp.where(mask, keep, 0.0)
-    tail = jnp.dot(upper, keep.astype(jnp.bfloat16), preferred_element_type=jnp.float32)
-    weights = jnp.exp2((scores - keep) - (tail + carry))
-    if mask is not None:
-        weights = jnp.where(mask, weights, 0.0)
-    part = jnp.dot(v_t, weights.astype(jnp.bfloat16), preferred_element_type=jnp.float32)
-    return part, carry + (tail[0:1] + keep[0:1])
+def sub_step(k, q, offset, carry, mask):
+    scores = jnp.dot(k, q, preferred_element_type=jnp.float32)
+    lanes = scores.shape[1]
+    sub = lax.broadcasted_iota(jnp.int32, (sublanes, lanes), 0)
+    kept, pieces = None, []
+    for i in range(scores.shape[0] // sublanes):
+        rows = slice(i * sublanes, (i + 1) * sublanes)
+        odds = jnp.exp2(scores[rows] + offset)
+        if mask is not None:
+            odds = jnp.where(mask[rows], odds, 0.0)
+        keep = 1.0 / (1.0 + odds)
+        piece = odds * keep
+        pieces.append(piece if kept is None else piece * kept)
+        kept = keep if kept is None else kept * keep
+    for j in (1, 2, 4):
+        kept = kept * jnp.where(sub < sublanes - j, pltpu.roll(kept, sublanes - j, 0), 1.0)
+    later = jnp.where(sub < sublanes - 1, pltpu.roll(kept, sublanes - 1, 0), 1.0) * carry
+    carry = carry * jnp.broadcast_to(kept[0:1], kept.shape)
+    weights = jnp.concatenate([piece * later for piece in pieces], axis=0)
+    return weights.astype(jnp.bfloat16), carry
+
+
+def block_step(k, v_t, q, offset, carry, mask):
+    half = tile // 2
+    upper, carry = sub_step(k[half:], q, offset, carry, None if mask is None else mask[half:])
+    lower, carry = sub_step(k[:half], q, offset, carry, None if mask is None else mask[:half])
+    part = jnp.dot(v_t[:, half:], upper, preferred_element_type=jnp.float32)
+    part += jnp.dot(v_t[:, :half], lower, preferred_element_type=jnp.float32)
+    return part, carry
 
 
 def attend_kernel(
-    place, offsets, w_own, w_left, w_right, w_low, w_high, x_own, x_core, x_far, x_both,
+    place, offsets, w_own, w_left, w_left_end, w_right, w_right_end, w_far, w_far_end, x_own, x_core, x_far, x_both,
     kv_own, kv_one, kv_two, kv_three, gain, out, q_rows, total, carries,
 ):
     part, chip, core, column = place[0], place[1], place[2], place[3]
@@ -35,9 +54,17 @@
     head_width = gain.shape[0]
     heads = offsets.shape[0]
     span = w_own.shape[0]
-    half_span = w_low.shape[0]
+    half_span = w_far.shape[0]
     queries = None
-    sources = ((w_own, 0, 0), (w_left, 3, 0), (w_right, 1, 0), (w_low, 2, 0), (w_high, 2, half_span))
+    sources = (
+        (w_own, 0, 0),
+        (w_left, 3, 0),
+        (w_left_end, 3, half_span),
+        (w_right, 1, 0),
+        (w_right_end, 1, half_span),
+        (w_far, 2, 0),
+        (w_far_end, 2, half_span),
+    )
     for weight, shift, begin in sources:
         start = pl.multiple_of(lax.rem(column + shift, low_x) * span + begin, 16)
         rows = pl.ds(start, weight.shape[0])
@@ -65,8 +92,11 @@
             q_rows[jnp.bitwise_xor(chip, t), h] = scaled.astype(jnp.bfloat16)
     row_id = lax.broadcasted_iota(jnp.int32, (tile, tile), 0)
     column_id = lax.broadcasted_iota(jnp.int32, (tile, tile), 1)
-    upper = (column_id > row_id).astype(jnp.float32).astype(jnp.bfloat16)
-    mask = row_id < column_id
+    half = tile // 2
+    inner = row_id % half
+    depth = half // sublanes
+    key_id = row_id - inner + (inner % sublanes) * depth + (depth - 1 - inner // sublanes)
+    mask = key_id < column_id
 
     def block_of(kv, index):
         left = kv[jnp.bitwise_xor(2 * index, member)]
@@ -74,17 +104,17 @@
         k = jnp.concatenate([left[0], right[0]], axis=0)
         return k, jnp.concatenate([left[1], right[1]], axis=1)
 
-    zero = jnp.zeros((1, tile), jnp.float32)
+    one = jnp.ones((sublanes, tile), jnp.float32)
     first, last = block_of(kv_own, 0), block_of(kv_own, 1)
     for h in range(heads):
         offset = offsets[h]
-        piece, carry = block_step(*last, q_rows[1, h], upper, offset, zero, mask)
-        more, carry = block_step(*first, q_rows[1, h], upper, offset, carry, None)
+        piece, carry = block_step(*last, q_rows[1, h], offset, one, mask)
+        more, carry = block_step(*first, q_rows[1, h], offset, carry, None)
         total[h, 1] = piece + more
-        carries[h, 1] = jnp.broadcast_to(carry, (8, tile))
-        piece, carry = block_step(*first, q_rows[0, h], upper, offset, zero, mask)
+        carries[h, 1] = carry
+        piece, carry = block_step(*first, q_rows[0, h], offset, one, mask)
         total[h, 0] = piece
-        carries[h, 0] = jnp.broadcast_to(carry, (8, tile))
+        carries[h, 0] = carry
 
     for distance, kv in ((1, kv_one), (2, kv_two), (3, kv_three)):
 
@@ -93,16 +123,15 @@
             blocks = (block_of(kv, 1), block_of(kv, 0))
             for h in range(heads):
                 for t in range(2):
-                    carry, summed = carries[h, t, 0:1], total[h, t]
+                    carry, summed = carries[h, t], total[h, t]
                     for k, v_t in blocks:
                         piece, carry = block_step(
-                            k, v_t, q_rows[t, h], upper, offsets[h], carry, None
+                            k, v_t, q_rows[t, h], offsets[h], carry, None
                         )
                         summed = summed + piece
                     total[h, t] = summed
-                    carries[h, t] = jnp.broadcast_to(carry, (8, tile))
-
-    half = tile // 2
+                    carries[h, t] = carry
+
     for h in range(heads):
         for t in range(2):
             rows = total[h, t].T.astype(jnp.bfloat16)
@@ -122,12 +151,12 @@
     return pl.pallas_call(
         attend_kernel,
         out_shape=jax.ShapeDtypeStruct((group, tile // 2, heads * head_width), jnp.bfloat16),
-        in_specs=[smem, smem, *[vmem] * 14],
+        in_specs=[smem, smem, *[vmem] * 16],
         out_specs=vmem,
         scratch_shapes=[
             pltpu.VMEM((2, heads, head_width, tile), jnp.bfloat16),
             pltpu.VMEM((heads, 2, head_width, tile), jnp.float32),
-            pltpu.VMEM((heads, 2, 8, tile), jnp.float32),
+            pltpu.VMEM((heads, 2, sublanes, tile), jnp.float32),
         ],
         cost_estimate=pl.CostEstimate(flops=flops, bytes_accessed=1 << 22, transcendentals=0),
     )(place, offsets, *weights, *xs, *kvs, gain)
@@ -173,10 +202,14 @@
     along_z = sent_to_all(columns, "z").reshape(-1, span)
 
     kv_heads = keys.shape[2] // head_width
-    k = keys[0].reshape(tokens, kv_heads, head_width).astype(jnp.float32)
+
+    def spread(rows):
+        return rows.reshape(sublanes, tokens // sublanes, -1)[:, ::-1].swapaxes(0, 1)
+
+    k = spread(keys[0]).reshape(tokens, kv_heads, head_width).astype(jnp.float32)
     k = k * lax.rsqrt(jnp.mean(k * k, axis=-1, keepdims=True) + norm_eps) * key_gain
     k = k.astype(jnp.bfloat16).transpose(1, 0, 2)
-    v = values[0].reshape(tokens, kv_heads, head_width).transpose(1, 2, 0)
+    v = spread(values[0]).reshape(tokens, kv_heads, head_width).transpose(1, 2, 0)
     kv = jnp.stack((k, v), axis=1)
     pieces = [lax.dynamic_index_in_dim(kv, member ^ bits, 0, keepdims=True) for bits in range(group)]
     pieces[1:] = [flipped(pieces[bits], bits) for bits in range(1, group)]
@@ -193,10 +226,15 @@
     near = swapped(normed, "core")
     xs = (normed, near, far, swapped(far, "core"))
 
-    left, right = turned(along_z, "x", 1), turned(along_z, "x", -1)
     half = along_z.shape[0] // 2
-    low, high = turned(left[:half], "x", 1), turned(right[half:], "x", -1)
-    weights = (along_z, left, right, low, high)
+    top, bottom = along_z[:half], along_z[half:]
+    left_top = turned(top, "x", 1)
+    right_bottom = turned(bottom, "x", -1)
+    left_bottom = turned(bottom, "x", 1)
+    right_top = turned(top, "x", -1)
+    far_top = turned(left_top, "x", 1)
+    far_bottom = turned(right_bottom, "x", -1)
+    weights = (along_z, left_top, left_bottom, right_top, right_bottom, far_top, far_bottom)
 
     gain = query_gain * (head_width ** (-0.5) * log2_e)
     gain = jnp.broadcast_to(gain[:, None], (head_width, head_width))

time: 146 us -> 134 us (0.918)
  the two profiles are of different devices: /device:TPU:112 before, /device:TPU:48 now
where the time goes in v2:
time: 134 us; the launch traced here: 133 us
  starting transfers between devices  55.3 us (41%)
  waiting for transfers between devices  43.5 us (32%)
  Pallas kernels  13 us (10%)
  blocking collectives  12.3 us (9%)
  local copies, waits for them, and re-layouts  6.75 us (5%)
  other arithmetic  1.66 us (1%)
    ppermute x3, waiting for transfers between devices, handed_on(): lax.ppermute(value, 'yh', [(i, i + shift) for i in range(count - shift)])  27.4 us
    ppermute x6, starting transfers between devices, turned(): lax.ppermute(value, axis, [(i, (i + shift) % count) for i in range(count)])  21.7 us
    all_to_all x1, starting transfers between devices, sent_to_all(): return lax.all_to_all(copies, axes, split_axis=0, concat_axis=0, tiled=True)  15.3 us
    pallas_call x1, Pallas kernels, attend(): pl.pallas_call(attend_kernel, out_shape=jax.ShapeDtypeStruct((group, tile...  13 us
    all_to_all x1, blocking collectives, layer(): lax.all_to_all(attended, ('yl', 'core'), split_axis=0, concat_axis=0, til...  12.3 us
    ppermute x6, waiting for transfers between devices, turned(): lax.ppermute(value, axis, [(i, (i + shift) % count) for i in range(count)])  8.44 us
    ppermute x3, starting transfers between devices, flipped(): lax.ppermute(value, ('yl', 'core'), [(i, i ^ bits) for i in range(group)])  7.59 us
    ppermute x3, starting transfers between devices, swapped(): return lax.ppermute(value, axis, [(0, 1), (1, 0)])  6.71 us
  transfers between devices with their start and end apart: 16, of which 6 were waited for; matrix products, arithmetic and copies ran while one was open for 2% of the time, Pallas kernels for 0%

profile of v2, /device:TPU:48, one launch (start us, length us, event | category | flops | bytes accessed | tf_op | source)
XLA Modules:
  0.0 133.0 jit_solution(12286804302634159655)
XLA Ops:
  0.0 0.9 copy-done
  0.9 0.9 broadcast_in_dim.4
  1.8 15.3 %all-to-all-start = ((bf16[12,48,512]{2,1,0:T(8,128)(2,1)}), bf16[12,48,512]{2,1,0:T(8,128)(2,1)S(1)}, u32[]{:S(2)}, u32[]{:S(2)}) async-start(bf16[12,48,512]{2,1,0:T(8,128)(2,1)} %broadcast_in_dim.4), calls=%async_computation | async-start | bytes 1179648 | tf_op jit(solution)/shard_map/all_to_all | solution.py:168
  17.1 0.3 fusion
  17.4 0.3 fusion.3
  17.8 0.2 reshape.42
  18.0 0.0 copy-start.5
  18.0 0.1 pad.9.clone
  18.1 2.6 %collective-permute-start.7 = (bf16[2304,128]{1,0:T(8,128)(2,1)S(1)}, bf16[2304,128]{1,0:T(8,128)(2,1)S(1)}, u32[]{:S(2)}, u32[]{:S(2)}) collective-permute-start(bf16[2304,128]{1,0:T(8,128)(2,1)S(1)} %bitcast.34), channel_id=1, source_target_pairs={{0,96},{96,0},{1,97},{97,1},{2,98},{98,2},{3,99},{99,3},{4,100},{1... | collective-permute-start | bytes 1769480 | tf_op jit(solution)/shard_map/ppermute | solution.py:172
  20.7 0.1 copy.27
  20.8 0.0 copy-start.6
  20.9 0.1 reshape.47
  21.0 0.2 multiply_reduce_fusion
  21.2 0.0 copy-start.8
  21.2 0.1 copy.28
  21.2 0.5 copy-done.6
  21.7 0.1 copy.30
  21.9 0.1 copy.31
  22.0 0.1 fusion.6
  22.2 1.9 %collective-permute-start.9 = (bf16[1,2,128,128]{3,2,1,0:T(8,128)(2,1)S(1)}, bf16[1,2,128,128]{3,2,1,0:T(8,128)(2,1)S(1)}, u32[]{:S(2)}, u32[]{:S(2)}) collective-permute-start(bf16[1,2,128,128]{3,2,1,0:T(8,128)(2,1)S(1)} %get-tuple-element.8), channel_id=1, source_target_pairs={{0,48},{48,0},{96,144},{144,96},{1,49},{49,1},{97,145},{145,97},{2... | collective-permute-start | bytes 196616 | tf_op jit(solution)/shard_map/ppermute | solution.py:181
  24.2 3.3 %collective-permute-start.10 = (bf16[1,2,128,128]{3,2,1,0:T(8,128)(2,1)S(1)}, bf16[1,2,128,128]{3,2,1,0:T(8,128)(2,1)S(1)}, u32[]{:S(2)}, u32[]{:S(2)}) collective-permute-start(bf16[1,2,128,128]{3,2,1,0:T(8,128)(2,1)S(1)} %get-tuple-element.9), channel_id=1, source_target_pairs={{0,96},{48,144},{96,0},{144,48},{1,97},{49,145},{97,1},{145,49},{2... | collective-permute-start | bytes 196616 | tf_op jit(solution)/shard_map/ppermute | solution.py:181
  27.4 2.4 %collective-permute-start.11 = (bf16[1,2,128,128]{3,2,1,0:T(8,128)(2,1)S(1)}, bf16[1,2,128,128]{3,2,1,0:T(8,128)(2,1)S(1)}, u32[]{:S(2)}, u32[]{:S(2)}) collective-permute-start(bf16[1,2,128,128]{3,2,1,0:T(8,128)(2,1)S(1)} %get-tuple-element.10), channel_id=1, source_target_pairs={{0,144},{48,96},{96,48},{144,0},{1,145},{49,97},{97,49},{145,1},{2... | collective-permute-start | bytes 196616 | tf_op jit(solution)/shard_map/ppermute | solution.py:181
  29.8 2.2 %collective-permute-start.6 = (bf16[2304,128]{1,0:T(8,128)(2,1)S(1)}, bf16[2304,128]{1,0:T(8,128)(2,1)S(1)}, u32[]{:S(2)}, u32[]{:S(2)}) collective-permute-start(bf16[2304,128]{1,0:T(8,128)(2,1)S(1)} %bitcast.35), channel_id=1, source_target_pairs={{0,48},{48,0},{1,49},{49,1},{2,50},{50,2},{3,51},{51,3},{4,52},{52... | collective-permute-start | bytes 1769480 | tf_op jit(solution)/shard_map/ppermute | solution.py:172
  32.1 4.8 %collective-permute-done.10 = bf16[1,2,128,128]{3,2,1,0:T(8,128)(2,1)S(1)} collective-permute-done((bf16[1,2,128,128]{3,2,1,0:T(8,128)(2,1)S(1)}, bf16[1,2,128,128]{3,2,1,0:T(8,128)(2,1)S(1)}, u32[]{:S(2)}, u32[]{:S(2)}) %collective-permute-start.10) | collective-permute-done | bytes 65568 | tf_op jit(solution)/shard_map/ppermute | solution.py:181
  37.0 1.4 %collective-permute-start.14 = (bf16[4,2,128,128]{3,2,1,0:T(8,128)(2,1)S(1)}, bf16[4,2,128,128]{3,2,1,0:T(8,128)(2,1)}, u32[]{:S(2)}, u32[]{:S(2)}) collective-permute-start(bf16[4,2,128,128]{3,2,1,0:T(8,128)(2,1)S(1)} %pad_maximum_fusion.kv_own), channel_id=1, source_target_pairs={{0,576},{1,577},{2,578},{3,579},{4,580},{5,581},{6,582},{7,583},{8... | collective-permute-start | bytes 786440 | tf_op jit(solution)/shard_map/ppermute | solution.py:186
  38.4 1.3 collective-permute-start.13
  39.7 2.8 %all-to-all-done = bf16[12,48,512]{2,1,0:T(8,128)(2,1)S(1)} async-done(((bf16[12,48,512]{2,1,0:T(8,128)(2,1)}), bf16[12,48,512]{2,1,0:T(8,128)(2,1)S(1)}, u32[]{:S(2)}, u32[]{:S(2)}) %all-to-all-start) | async-done | bytes 589856 | tf_op jit(solution)/shard_map/all_to_all | solution.py:168
  42.6 0.8 copy-done.1
  43.4 3.4 %collective-permute-start = (bf16[288,512]{1,0:T(8,128)(2,1)S(1)}, bf16[288,512]{1,0:T(8,128)(2,1)}, u32[]{:S(2)}, u32[]{:S(2)}) collective-permute-start(bf16[288,512]{1,0:T(8,128)(2,1)S(1)} %bitcast.40), channel_id=1, source_target_pairs={{0,1},{1,2},{2,3},{3,0},{4,5},{5,6},{6,7},{7,4},{8,9},{9,10},{10,1... | collective-permute-start | bytes 884744 | tf_op jit(solution)/shard_map/ppermute | solution.py:177
  46.8 20.0 %collective-permute-done.14.kv_three = bf16[4,2,128,128]{3,2,1,0:T(8,128)(2,1)} collective-permute-done((bf16[4,2,128,128]{3,2,1,0:T(8,128)(2,1)S(1)}, bf16[4,2,128,128]{3,2,1,0:T(8,128)(2,1)}, u32[]{:S(2)}, u32[]{:S(2)}) %collective-permute-start.14) | collective-permute-done | bytes 262176 | tf_op jit(solution)/shard_map/ppermute | solution.py:186
  66.8 4.7 %collective-permute-start.3 = (bf16[288,512]{1,0:T(8,128)(2,1)S(1)}, bf16[288,512]{1,0:T(8,128)(2,1)}, u32[]{:S(2)}, u32[]{:S(2)}) collective-permute-start(bf16[288,512]{1,0:T(8,128)(2,1)S(1)} %bitcast.38), channel_id=1, source_target_pairs={{0,3},{1,0},{2,1},{3,2},{4,7},{5,4},{6,5},{7,6},{8,11},{9,8},{10,9... | collective-permute-start | bytes 884744 | tf_op jit(solution)/shard_map/ppermute | solution.py:177
  71.5 1.3 collective-permute-start.12
  72.8 1.9 %collective-permute-start.8 = (bf16[2304,128]{1,0:T(8,128)(2,1)S(1)}, bf16[2304,128]{1,0:T(8,128)(2,1)S(1)}, u32[]{:S(2)}, u32[]{:S(2)}) collective-permute-start(bf16[2304,128]{1,0:T(8,128)(2,1)S(1)} %collective-permute-done.7.x_far), channel_id=1, source_target_pairs={{0,48},{48,0},{1,49},{49,1},{2,50},{50,2},{3,51},{51,3},{4,52},{52... | collective-permute-start | bytes 1769480 | tf_op jit(solution)/shard_map/ppermute | solution.py:172
  74.8 0.7 dynamic_slice.19.offsets
  75.4 7.4 %collective-permute-done.12.kv_one = bf16[4,2,128,128]{3,2,1,0:T(8,128)(2,1)} collective-permute-done((bf16[4,2,128,128]{3,2,1,0:T(8,128)(2,1)S(1)}, bf16[4,2,128,128]{3,2,1,0:T(8,128)(2,1)}, u32[]{:S(2)}, u32[]{:S(2)}) %collective-permute-start.12) | collective-permute-done | bytes 262176 | tf_op jit(solution)/shard_map/ppermute | solution.py:186
  82.8 4.7 %collective-permute-start.2 = (bf16[288,512]{1,0:T(8,128)(2,1)S(1)}, bf16[288,512]{1,0:T(8,128)(2,1)S(1)}, u32[]{:S(2)}, u32[]{:S(2)}) collective-permute-start(bf16[288,512]{1,0:T(8,128)(2,1)S(1)} %bitcast.41), channel_id=1, source_target_pairs={{0,3},{1,0},{2,1},{3,2},{4,7},{5,4},{6,5},{7,6},{8,11},{9,8},{10,9... | collective-permute-start | bytes 884744 | tf_op jit(solution)/shard_map/ppermute | solution.py:177
  87.5 1.9 %collective-permute-start.1 = (bf16[288,512]{1,0:T(8,128)(2,1)S(1)}, bf16[288,512]{1,0:T(8,128)(2,1)S(1)}, u32[]{:S(2)}, u32[]{:S(2)}) collective-permute-start(bf16[288,512]{1,0:T(8,128)(2,1)S(1)} %bitcast.39), channel_id=1, source_target_pairs={{0,1},{1,2},{2,3},{3,0},{4,5},{5,6},{6,7},{7,4},{8,9},{9,10},{10,1... | collective-permute-start | bytes 884744 | tf_op jit(solution)/shard_map/ppermute | solution.py:177
  89.4 2.7 %collective-permute-start.4 = (bf16[288,512]{1,0:T(8,128)(2,1)}, bf16[288,512]{1,0:T(8,128)(2,1)S(1)}, u32[]{:S(2)}, u32[]{:S(2)}) collective-permute-start(bf16[288,512]{1,0:T(8,128)(2,1)} %collective-permute-done.w_left), channel_id=1, source_target_pairs={{0,1},{1,2},{2,3},{3,0},{4,5},{5,6},{6,7},{7,4},{8,9},{9,10},{10,1... | collective-permute-start | bytes 884744 | tf_op jit(solution)/shard_map/ppermute | solution.py:177
  92.1 4.4 %collective-permute-start.5 = (bf16[288,512]{1,0:T(8,128)(2,1)}, bf16[288,512]{1,0:T(8,128)(2,1)S(1)}, u32[]{:S(2)}, u32[]{:S(2)}) collective-permute-start(bf16[288,512]{1,0:T(8,128)(2,1)} %collective-permute-done.3.w_right_end), channel_id=1, source_target_pairs={{0,3},{1,0},{2,1},{3,2},{4,7},{5,4},{6,5},{7,6},{8,11},{9,8},{10,9... | collective-permute-start | bytes 884744 | tf_op jit(solution)/shard_map/ppermute | solution.py:177
  96.5 0.6 pad_add_fusion.place
  97.1 3.3 %collective-permute-done.1.w_left_end = bf16[288,512]{1,0:T(8,128)(2,1)S(1)} collective-permute-done((bf16[288,512]{1,0:T(8,128)(2,1)S(1)}, bf16[288,512]{1,0:T(8,128)(2,1)S(1)}, u32[]{:S(2)}, u32[]{:S(2)}) %collective-permute-start.1) | collective-permute-done | bytes 294944 | tf_op jit(solution)/shard_map/ppermute | solution.py:177
  100.5 5.1 %collective-permute-done.4.w_far = bf16[288,512]{1,0:T(8,128)(2,1)S(1)} collective-permute-done((bf16[288,512]{1,0:T(8,128)(2,1)}, bf16[288,512]{1,0:T(8,128)(2,1)S(1)}, u32[]{:S(2)}, u32[]{:S(2)}) %collective-permute-start.4) | collective-permute-done | bytes 294944 | tf_op jit(solution)/shard_map/ppermute | solution.py:177
  105.6 0.8 broadcast_in_dim.5.gain
  106.4 0.0 copy-done.15
  106.4 13.0 %shard_map.82 = bf16[4,128,512]{2,1,0:T(8,128)(2,1)} custom-call(s32[4]{0:T(128)} %pad_add_fusion.place, f32[4]{0:T(128)} %dynamic_slice.19.offsets, bf16[576,512]{1,0:T(8,128)(2,1)} %bitcast.30, bf16[288,512]{1,0:T(8,128)(2,1)} %collective-permute-done.w_left, bf16[288,512]{1,0:T(8,128)(2,1)} %copy-done.13, bf16[288,512]{1,0:T(8,128)(2,1)} %copy-done.12, ...), custom_call_target="tpu_custom_call" | custom-call | flops 3355443200 | bytes 4194304 | tf_op jit(solution)/shard_map/pallas_call | solution.py:151
  119.5 12.3 %all_to_all.10 = bf16[4,128,512]{2,1,0:T(8,128)(2,1)S(1)} all-to-all(bf16[4,128,512]{2,1,0:T(8,128)(2,1)} %shard_map.82), channel_id=1, replica_groups=mesh['yh'=4,'yl'=2,'core'=2,'z'=12,'x'=4] {'yl','core'}, dimensions={0} | all-to-all | bytes 1048576 | tf_op jit(solution)/shard_map/all_to_all | solution.py:244
  131.7 0.3 copy.32
  132.0 1.0 copy.33
  (52 shorter events, 0.3 us)
Async XLA Ops:
  0.0 0.9 copy-start
  1.8 15.3 %copy-start.2 = (bf16[1,128,2064]{1,2,0:T(8,128)(2,1)S(1)}, bf16[1,128,2064]{1,2,0:T(8,128)(2,1)}, u32[]{:S(2)}) copy-start(bf16[1,128,2064]{1,2,0:T(8,128)(2,1)} %param.8) | copy-start | bytes 1585156
  1.8 15.6 %copy-start.7 = (f32[2064]{0:T(1024)S(1)}, f32[2064]{0:T(1024)}, u32[]{:S(2)}) copy-start(f32[2064]{0:T(1024)} %param.9) | copy-start | bytes 24772
  1.8 40.7 %all-to-all-start = ((bf16[12,48,512]{2,1,0:T(8,128)(2,1)}), bf16[12,48,512]{2,1,0:T(8,128)(2,1)S(1)}, u32[]{:S(2)}, u32[]{:S(2)}) async-start(bf16[12,48,512]{2,1,0:T(8,128)(2,1)} %broadcast_in_dim.4), calls=%async_computation | async-start | bytes 1179648 | tf_op jit(solution)/shard_map/all_to_all | solution.py:168
  18.0 2.7 %copy-start.5 = (bf16[1,128,512]{2,1,0:T(8,128)(2,1)S(1)}, bf16[1,128,512]{2,1,0:T(8,128)(2,1)}, u32[]{:S(2)}) copy-start(bf16[1,128,512]{2,1,0:T(8,128)(2,1)} %param.12) | copy-start | bytes 393220
  18.1 11.7 %copy-start.3 = (bf16[4,12,48,128]{3,2,1,0:T(8,128)(2,1)}, bf16[4,12,48,128]{3,2,1,0:T(8,128)(2,1)S(1)}, u32[]{:S(2)}) copy-start(bf16[4,12,48,128]{3,2,1,0:T(8,128)(2,1)S(1)} %pad.9.clone) | copy-start | bytes 1769476
  18.1 54.7 %collective-permute-start.7 = (bf16[2304,128]{1,0:T(8,128)(2,1)S(1)}, bf16[2304,128]{1,0:T(8,128)(2,1)S(1)}, u32[]{:S(2)}, u32[]{:S(2)}) collective-permute-start(bf16[2304,128]{1,0:T(8,128)(2,1)S(1)} %bitcast.34), channel_id=1, source_target_pairs={{0,96},{96,0},{1,97},{97,1},{2,98},{98,2},{3,99},{99,3},{4,100},{1... | collective-permute-start | bytes 1769480 | tf_op jit(solution)/shard_map/ppermute | solution.py:172
  20.8 0.9 copy-start.6
  21.2 0.9 copy-start.8
  22.2 9.8 %collective-permute-start.9 = (bf16[1,2,128,128]{3,2,1,0:T(8,128)(2,1)S(1)}, bf16[1,2,128,128]{3,2,1,0:T(8,128)(2,1)S(1)}, u32[]{:S(2)}, u32[]{:S(2)}) collective-permute-start(bf16[1,2,128,128]{3,2,1,0:T(8,128)(2,1)S(1)} %get-tuple-element.8), channel_id=1, source_target_pairs={{0,48},{48,0},{96,144},{144,96},{1,49},{49,1},{97,145},{145,97},{2... | collective-permute-start | bytes 196616 | tf_op jit(solution)/shard_map/ppermute | solution.py:181
  24.2 12.7 %collective-permute-start.10 = (bf16[1,2,128,128]{3,2,1,0:T(8,128)(2,1)S(1)}, bf16[1,2,128,128]{3,2,1,0:T(8,128)(2,1)S(1)}, u32[]{:S(2)}, u32[]{:S(2)}) collective-permute-start(bf16[1,2,128,128]{3,2,1,0:T(8,128)(2,1)S(1)} %get-tuple-element.9), channel_id=1, source_target_pairs={{0,96},{48,144},{96,0},{144,48},{1,97},{49,145},{97,1},{145,49},{2... | collective-permute-start | bytes 196616 | tf_op jit(solution)/shard_map/ppermute | solution.py:181
  27.4 9.5 %collective-permute-start.11 = (bf16[1,2,128,128]{3,2,1,0:T(8,128)(2,1)S(1)}, bf16[1,2,128,128]{3,2,1,0:T(8,128)(2,1)S(1)}, u32[]{:S(2)}, u32[]{:S(2)}) collective-permute-start(bf16[1,2,128,128]{3,2,1,0:T(8,128)(2,1)S(1)} %get-tuple-element.10), channel_id=1, source_target_pairs={{0,144},{48,96},{96,48},{144,0},{1,145},{49,97},{97,49},{145,1},{2... | collective-permute-start | bytes 196616 | tf_op jit(solution)/shard_map/ppermute | solution.py:181
  29.8 57.6 %collective-permute-start.6 = (bf16[2304,128]{1,0:T(8,128)(2,1)S(1)}, bf16[2304,128]{1,0:T(8,128)(2,1)S(1)}, u32[]{:S(2)}, u32[]{:S(2)}) collective-permute-start(bf16[2304,128]{1,0:T(8,128)(2,1)S(1)} %bitcast.35), channel_id=1, source_target_pairs={{0,48},{48,0},{1,49},{49,1},{2,50},{50,2},{3,51},{51,3},{4,52},{52... | collective-permute-start | bytes 1769480 | tf_op jit(solution)/shard_map/ppermute | solution.py:172
  36.9 34.5 %copy-start.4 = (bf16[4,2,128,128]{3,2,1,0:T(8,128)(2,1)}, bf16[4,2,128,128]{3,2,1,0:T(8,128)(2,1)S(1)}, u32[]{:S(2)}) copy-start(bf16[4,2,128,128]{3,2,1,0:T(8,128)(2,1)S(1)} %pad_maximum_fusion.kv_own) | copy-start | bytes 786436
  36.9 37.8 %copy-start.16 = (f32[16]{0:T(128)S(1)}, f32[16]{0:T(128)}, u32[]{:S(2)}) copy-start(f32[16]{0:T(128)} %param.15) | copy-start | bytes 196
  37.0 60.1 %copy-start.17 = (f32[128]{0:T(128)S(1)}, f32[128]{0:T(128)}, u32[]{:S(2)}) copy-start(f32[128]{0:T(128)} %param.11) | copy-start | bytes 1540
  37.0 29.8 %collective-permute-start.14 = (bf16[4,2,128,128]{3,2,1,0:T(8,128)(2,1)S(1)}, bf16[4,2,128,128]{3,2,1,0:T(8,128)(2,1)}, u32[]{:S(2)}, u32[]{:S(2)}) collective-permute-start(bf16[4,2,128,128]{3,2,1,0:T(8,128)(2,1)S(1)} %pad_maximum_fusion.kv_own), channel_id=1, source_target_pairs={{0,576},{1,577},{2,578},{3,579},{4,580},{5,581},{6,582},{7,583},{8... | collective-permute-start | bytes 786440 | tf_op jit(solution)/shard_map/ppermute | solution.py:186
  38.4 33.1 %collective-permute-start.13 = (bf16[4,2,128,128]{3,2,1,0:T(8,128)(2,1)S(1)}, bf16[4,2,128,128]{3,2,1,0:T(8,128)(2,1)}, u32[]{:S(2)}, u32[]{:S(2)}) collective-permute-start(bf16[4,2,128,128]{3,2,1,0:T(8,128)(2,1)S(1)} %pad_maximum_fusion.kv_own), channel_id=1, source_target_pairs={{0,384},{192,576},{1,385},{193,577},{2,386},{194,578},{3,387},{195... | collective-permute-start | bytes 786440 | tf_op jit(solution)/shard_map/ppermute | solution.py:186
  42.5 0.8 copy-start.1
  43.4 46.1 %collective-permute-start = (bf16[288,512]{1,0:T(8,128)(2,1)S(1)}, bf16[288,512]{1,0:T(8,128)(2,1)}, u32[]{:S(2)}, u32[]{:S(2)}) collective-permute-start(bf16[288,512]{1,0:T(8,128)(2,1)S(1)} %bitcast.40), channel_id=1, source_target_pairs={{0,1},{1,2},{2,3},{3,0},{4,5},{5,6},{6,7},{7,4},{8,9},{9,10},{10,1... | collective-permute-start | bytes 884744 | tf_op jit(solution)/shard_map/ppermute | solution.py:177
  66.8 25.3 %collective-permute-start.3 = (bf16[288,512]{1,0:T(8,128)(2,1)S(1)}, bf16[288,512]{1,0:T(8,128)(2,1)}, u32[]{:S(2)}, u32[]{:S(2)}) collective-permute-start(bf16[288,512]{1,0:T(8,128)(2,1)S(1)} %bitcast.38), channel_id=1, source_target_pairs={{0,3},{1,0},{2,1},{3,2},{4,7},{5,4},{6,5},{7,6},{8,11},{9,8},{10,9... | collective-permute-start | bytes 884744 | tf_op jit(solution)/shard_map/ppermute | solution.py:177
  71.5 11.3 %collective-permute-start.12 = (bf16[4,2,128,128]{3,2,1,0:T(8,128)(2,1)S(1)}, bf16[4,2,128,128]{3,2,1,0:T(8,128)(2,1)}, u32[]{:S(2)}, u32[]{:S(2)}) collective-permute-start(bf16[4,2,128,128]{3,2,1,0:T(8,128)(2,1)S(1)} %pad_maximum_fusion.kv_own), channel_id=1, source_target_pairs={{0,192},{192,384},{384,576},{1,193},{193,385},{385,577},{2,194},{1... | collective-permute-start | bytes 786440 | tf_op jit(solution)/shard_map/ppermute | solution.py:186
  72.8 33.6 %copy-start.9 = (bf16[2304,128]{1,0:T(8,128)(2,1)}, bf16[2304,128]{1,0:T(8,128)(2,1)S(1)}, u32[]{:S(2)}) copy-start(bf16[2304,128]{1,0:T(8,128)(2,1)S(1)} %collective-permute-done.7.x_far) | copy-start | bytes 1769476
  72.8 24.3 %collective-permute-start.8 = (bf16[2304,128]{1,0:T(8,128)(2,1)S(1)}, bf16[2304,128]{1,0:T(8,128)(2,1)S(1)}, u32[]{:S(2)}, u32[]{:S(2)}) collective-permute-start(bf16[2304,128]{1,0:T(8,128)(2,1)S(1)} %collective-permute-done.7.x_far), channel_id=1, source_target_pairs={{0,48},{48,0},{1,49},{49,1},{2,50},{50,2},{3,51},{51,3},{4,52},{52... | collective-permute-start | bytes 1769480 | tf_op jit(solution)/shard_map/ppermute | solution.py:172
  82.8 14.3 %collective-permute-start.2 = (bf16[288,512]{1,0:T(8,128)(2,1)S(1)}, bf16[288,512]{1,0:T(8,128)(2,1)S(1)}, u32[]{:S(2)}, u32[]{:S(2)}) collective-permute-start(bf16[288,512]{1,0:T(8,128)(2,1)S(1)} %bitcast.41), channel_id=1, source_target_pairs={{0,3},{1,0},{2,1},{3,2},{4,7},{5,4},{6,5},{7,6},{8,11},{9,8},{10,9... | collective-permute-start | bytes 884744 | tf_op jit(solution)/shard_map/ppermute | solution.py:177
  87.5 18.9 %copy-start.10 = (bf16[2304,128]{1,0:T(8,128)(2,1)}, bf16[2304,128]{1,0:T(8,128)(2,1)S(1)}, u32[]{:S(2)}) copy-start(bf16[2304,128]{1,0:T(8,128)(2,1)S(1)} %collective-permute-done.6.x_core) | copy-start | bytes 1769476
  87.5 13.0 %collective-permute-start.1 = (bf16[288,512]{1,0:T(8,128)(2,1)S(1)}, bf16[288,512]{1,0:T(8,128)(2,1)S(1)}, u32[]{:S(2)}, u32[]{:S(2)}) collective-permute-start(bf16[288,512]{1,0:T(8,128)(2,1)S(1)} %bitcast.39), channel_id=1, source_target_pairs={{0,1},{1,2},{2,3},{3,0},{4,5},{5,6},{6,7},{7,4},{8,9},{9,10},{10,1... | collective-permute-start | bytes 884744 | tf_op jit(solution)/shard_map/ppermute | solution.py:177
  89.4 16.1 %collective-permute-start.4 = (bf16[288,512]{1,0:T(8,128)(2,1)}, bf16[288,512]{1,0:T(8,128)(2,1)S(1)}, u32[]{:S(2)}, u32[]{:S(2)}) collective-permute-start(bf16[288,512]{1,0:T(8,128)(2,1)} %collective-permute-done.w_left), channel_id=1, source_target_pairs={{0,1},{1,2},{2,3},{3,0},{4,5},{5,6},{6,7},{7,4},{8,9},{9,10},{10,1... | collective-permute-start | bytes 884744 | tf_op jit(solution)/shard_map/ppermute | solution.py:177
  92.1 13.5 %collective-permute-start.5 = (bf16[288,512]{1,0:T(8,128)(2,1)}, bf16[288,512]{1,0:T(8,128)(2,1)S(1)}, u32[]{:S(2)}, u32[]{:S(2)}) collective-permute-start(bf16[288,512]{1,0:T(8,128)(2,1)} %collective-permute-done.3.w_right_end), channel_id=1, source_target_pairs={{0,3},{1,0},{2,1},{3,2},{4,7},{5,4},{6,5},{7,6},{8,11},{9,8},{10,9... | collective-permute-start | bytes 884744 | tf_op jit(solution)/shard_map/ppermute | solution.py:177
  97.1 9.3 %copy-start.11 = (bf16[2304,128]{1,0:T(8,128)(2,1)}, bf16[2304,128]{1,0:T(8,128)(2,1)S(1)}, u32[]{:S(2)}) copy-start(bf16[2304,128]{1,0:T(8,128)(2,1)S(1)} %collective-permute-done.8.x_both) | copy-start | bytes 1769476
  97.1 9.3 %copy-start.12 = (bf16[288,512]{1,0:T(8,128)(2,1)}, bf16[288,512]{1,0:T(8,128)(2,1)S(1)}, u32[]{:S(2)}) copy-start(bf16[288,512]{1,0:T(8,128)(2,1)S(1)} %collective-permute-done.2.w_right) | copy-start | bytes 884740
  100.5 5.9 %copy-start.13 = (bf16[288,512]{1,0:T(8,128)(2,1)}, bf16[288,512]{1,0:T(8,128)(2,1)S(1)}, u32[]{:S(2)}) copy-start(bf16[288,512]{1,0:T(8,128)(2,1)S(1)} %collective-permute-done.1.w_left_end) | copy-start | bytes 884740
  105.6 0.8 copy-start.14
  105.6 0.8 copy-start.15

commit v3 on v2

--- a/solution.py
+++ b/solution.py
@@ -45,17 +45,66 @@
     return part, carry
 
 
-def attend_kernel(
-    place, offsets, w_own, w_left, w_left_end, w_right, w_right_end, w_far, w_far_end, x_own, x_core, x_far, x_both,
-    kv_own, kv_one, kv_two, kv_three, gain, out, q_rows, total, carries,
+def attend_rows(late, place, offsets, q_rows, kvs, arrivals, out, total, carries):
+    part, core, member = place[0], place[1], place[3]
+    heads, head_width = q_rows.shape[:2]
+    half = tile // 2
+    row_id = lax.broadcasted_iota(jnp.int32, (tile, tile), 0)
+    column_id = lax.broadcasted_iota(jnp.int32, (tile, tile), 1)
+    inner = row_id % half
+    depth = half // sublanes
+    key_id = row_id - inner + (inner % sublanes) * depth + (depth - 1 - inner // sublanes)
+
+    def block_of(distance, index):
+        left = kvs[distance, jnp.bitwise_xor(2 * index, member)]
+        right = kvs[distance, jnp.bitwise_xor(2 * index + 1, member)]
+        k = jnp.concatenate([left[0], right[0]], axis=0)
+        return k, jnp.concatenate([left[1], right[1]], axis=1)
+
+    def walk(blocks, mask):
+        for h in range(heads):
+            carry, summed = carries[h], total[h]
+            for k, v_t in blocks:
+                piece, carry = block_step(k, v_t, q_rows[h], offsets[h], carry, mask)
+                summed = summed + piece
+            total[h] = summed
+            carries[h] = carry
+
+    for h in range(heads):
+        total[h] = jnp.zeros((head_width, tile), jnp.float32)
+        carries[h] = jnp.ones((sublanes, tile), jnp.float32)
+    arrivals[0].wait()
+
+    @pl.when(late == 1)
+    def _():
+        walk([block_of(0, 1)], key_id < column_id)
+
+    walk([block_of(0, 0)], key_id < column_id + late * tile)
+    for distance in range(1, kvs.shape[0]):
+        arrivals[distance].wait()
+
+        @pl.when(part >= distance)
+        def _(distance=distance):
+            walk([block_of(distance, 1), block_of(distance, 0)], None)
+
+    for h in range(heads):
+        turned_back = total[h].T.astype(jnp.bfloat16)
+        for c in range(cores):
+            out[jnp.bitwise_xor(core, c), :, h * head_width : (h + 1) * head_width] = turned_back[
+                c * half : (c + 1) * half
+            ]
+
+
+def first_kernel(
+    place, offsets, w_own, w_left, w_left_end, w_right, w_right_end, w_far, w_far_end,
+    x_far, x_both, x_own, x_near, kv_own, kv_one, kv_two, kv_three, gain,
+    out, q_mine, q_rows, weight, rows, kvs, total, carries, done,
 ):
-    part, chip, core, column = place[0], place[1], place[2], place[3]
-    member = chip * cores + core
-    head_width = gain.shape[0]
-    heads = offsets.shape[0]
+    core, column = place[1], place[2]
+    heads, head_width = q_rows.shape[:2]
     span = w_own.shape[0]
     half_span = w_far.shape[0]
-    queries = None
+    half = tile // 2
     sources = (
         (w_own, 0, 0),
         (w_left, 3, 0),
@@ -65,101 +114,100 @@
         (w_far, 2, 0),
         (w_far_end, 2, half_span),
     )
-    for weight, shift, begin in sources:
+    moves = []
+    for n, piece in enumerate((x_far, x_both, x_own, x_near)):
+        place_at = (n // 2) * tile + jnp.bitwise_xor(core, n % 2) * half
+        moves.append((piece, rows.at[:, pl.ds(pl.multiple_of(place_at, half), half)]))
+    for piece, shift, begin in sources:
         start = pl.multiple_of(lax.rem(column + shift, low_x) * span + begin, 16)
-        rows = pl.ds(start, weight.shape[0])
-        own, near, far, both = x_own[rows], x_core[rows], x_far[rows], x_both[rows]
-        flip = core == 0
-        wide = jnp.concatenate(
-            [
-                jnp.where(flip, own, near),
-                jnp.where(flip, near, own),
-                jnp.where(flip, far, both),
-                jnp.where(flip, both, far),
-            ],
-            axis=1,
-        )
-        term = lax.dot_general(
-            weight[...], wide, (((0,), (0,)), ((), ())), preferred_element_type=jnp.float32
-        )
-        queries = term if queries is None else queries + term
+        moves.append((piece, weight.at[pl.ds(start, piece.shape[0])]))
+    first_kv = len(moves)
+    for n, piece in enumerate((kv_own, kv_one, kv_two, kv_three)):
+        moves.append((piece, kvs.at[n]))
+    moves = [pltpu.make_async_copy(a, b, done.at[n]) for n, (a, b) in enumerate(moves)]
+    for move in moves:
+        move.start()
+    for move in moves[:first_kv]:
+        move.wait()
+    queries = lax.dot_general(
+        weight[...], rows[...], (((0,), (0,)), ((), ())), preferred_element_type=jnp.float32
+    )
     for h in range(heads):
-        for t in range(2):
-            rows = queries[h * head_width : (h + 1) * head_width, t * tile : (t + 1) * tile]
-            rows = rows.astype(jnp.bfloat16).astype(jnp.float32)
-            mean = jnp.mean(rows * rows, axis=0, keepdims=True)
-            scaled = rows * lax.rsqrt(mean + norm_eps) * gain[:, 0:1]
-            q_rows[jnp.bitwise_xor(chip, t), h] = scaled.astype(jnp.bfloat16)
-    row_id = lax.broadcasted_iota(jnp.int32, (tile, tile), 0)
-    column_id = lax.broadcasted_iota(jnp.int32, (tile, tile), 1)
-    half = tile // 2
-    inner = row_id % half
-    depth = half // sublanes
-    key_id = row_id - inner + (inner % sublanes) * depth + (depth - 1 - inner // sublanes)
-    mask = key_id < column_id
-
-    def block_of(kv, index):
-        left = kv[jnp.bitwise_xor(2 * index, member)]
-        right = kv[jnp.bitwise_xor(2 * index + 1, member)]
-        k = jnp.concatenate([left[0], right[0]], axis=0)
-        return k, jnp.concatenate([left[1], right[1]], axis=1)
-
-    one = jnp.ones((sublanes, tile), jnp.float32)
-    first, last = block_of(kv_own, 0), block_of(kv_own, 1)
-    for h in range(heads):
-        offset = offsets[h]
-        piece, carry = block_step(*last, q_rows[1, h], offset, one, mask)
-        more, carry = block_step(*first, q_rows[1, h], offset, carry, None)
-        total[h, 1] = piece + more
-        carries[h, 1] = carry
-        piece, carry = block_step(*first, q_rows[0, h], offset, one, mask)
-        total[h, 0] = piece
-        carries[h, 0] = carry
-
-    for distance, kv in ((1, kv_one), (2, kv_two), (3, kv_three)):
-
-        @pl.when(part >= distance)
-        def _(kv=kv):
-            blocks = (block_of(kv, 1), block_of(kv, 0))
-            for h in range(heads):
-                for t in range(2):
-                    carry, summed = carries[h, t], total[h, t]
-                    for k, v_t in blocks:
-                        piece, carry = block_step(
-                            k, v_t, q_rows[t, h], offsets[h], carry, None
-                        )
-                        summed = summed + piece
-                    total[h, t] = summed
-                    carries[h, t] = carry
-
-    for h in range(heads):
-        for t in range(2):
-            rows = total[h, t].T.astype(jnp.bfloat16)
-            for c in range(2):
-                out[2 * t + c, :, h * head_width : (h + 1) * head_width] = rows[
-                    c * half : (c + 1) * half
-                ]
-
-
-def attend(place, offsets, weights, xs, kvs, gain):
+        for side, target in enumerate((q_rows, q_mine)):
+            wide = queries[h * head_width : (h + 1) * head_width, side * tile : (side + 1) * tile]
+            wide = wide.astype(jnp.bfloat16).astype(jnp.float32)
+            mean = jnp.mean(wide * wide, axis=0, keepdims=True)
+            scaled = wide * lax.rsqrt(mean + norm_eps) * gain[:, 0:1]
+            target[h] = scaled.astype(jnp.bfloat16)
+    late = 1 - place[4]
+    attend_rows(late, place, offsets, q_rows, kvs, moves[first_kv:], out, total, carries)
+
+
+def second_kernel(
+    place, offsets, q_rows, kv_own, kv_one, kv_two, kv_three, out, kvs, total, carries, done
+):
+    moves = [
+        pltpu.make_async_copy(piece, kvs.at[n], done.at[n])
+        for n, piece in enumerate((kv_own, kv_one, kv_two, kv_three))
+    ]
+    for move in moves:
+        move.start()
+    attend_rows(place[4], place, offsets, q_rows, kvs, moves, out, total, carries)
+
+
+vmem = pl.BlockSpec(memory_space=pltpu.VMEM)
+smem = pl.BlockSpec(memory_space=pltpu.SMEM)
+anywhere = pl.BlockSpec(memory_space=pl.ANY)
+
+
+def estimate(heads, head_width, features):
+    flops = 2 * features * 2 * tile * heads * head_width
+    flops += heads * 8 * tile * tile * 4 * head_width
+    return pl.CostEstimate(flops=flops, bytes_accessed=1 << 22, transcendentals=0)
+
+
+def attend_first(place, offsets, weights, xs, kvs, gain):
     heads = offsets.shape[0]
     head_width = gain.shape[0]
-    vmem = pl.BlockSpec(memory_space=pltpu.VMEM)
-    smem = pl.BlockSpec(memory_space=pltpu.SMEM)
-    flops = 2 * xs[0].size * heads * head_width * group
-    flops += heads * 8 * 2 * tile * tile * (2 * head_width + tile)
+    features = xs[0].shape[0]
+    moved = len(weights) + len(xs) + len(kvs)
+    q_shape = (heads, head_width, tile)
     return pl.pallas_call(
-        attend_kernel,
-        out_shape=jax.ShapeDtypeStruct((group, tile // 2, heads * head_width), jnp.bfloat16),
-        in_specs=[smem, smem, *[vmem] * 16],
+        first_kernel,
+        out_shape=(
+            jax.ShapeDtypeStruct((cores, tile // 2, heads * head_width), jnp.bfloat16),
+            jax.ShapeDtypeStruct(q_shape, jnp.bfloat16),
+        ),
+        in_specs=[smem, smem, *[anywhere] * moved, vmem],
+        out_specs=(vmem, vmem),
+        scratch_shapes=[
+            pltpu.VMEM(q_shape, jnp.bfloat16),
+            pltpu.VMEM((features, heads * head_width), jnp.bfloat16),
+            pltpu.VMEM((features, 2 * tile), jnp.bfloat16),
+            pltpu.VMEM((len(kvs), *kvs[0].shape), jnp.bfloat16),
+            pltpu.VMEM(q_shape, jnp.float32),
+            pltpu.VMEM((heads, sublanes, tile), jnp.float32),
+            pltpu.SemaphoreType.DMA((moved,)),
+        ],
+        cost_estimate=estimate(heads, head_width, features),
+    )(place, offsets, *weights, *xs, *kvs, gain)
+
+
+def attend_second(place, offsets, q_mine, kvs):
+    heads, head_width = q_mine.shape[:2]
+    return pl.pallas_call(
+        second_kernel,
+        out_shape=jax.ShapeDtypeStruct((cores, tile // 2, heads * head_width), jnp.bfloat16),
+        in_specs=[smem, smem, vmem, *[anywhere] * len(kvs)],
         out_specs=vmem,
         scratch_shapes=[
-            pltpu.VMEM((2, heads, head_width, tile), jnp.bfloat16),
-            pltpu.VMEM((heads, 2, head_width, tile), jnp.float32),
-            pltpu.VMEM((heads, 2, sublanes, tile), jnp.float32),
+            pltpu.VMEM((len(kvs), *kvs[0].shape), jnp.bfloat16),
+            pltpu.VMEM(q_mine.shape, jnp.float32),
+            pltpu.VMEM((heads, sublanes, tile), jnp.float32),
+            pltpu.SemaphoreType.DMA((len(kvs),)),
         ],
-        cost_estimate=pl.CostEstimate(flops=flops, bytes_accessed=1 << 22, transcendentals=0),
-    )(place, offsets, *weights, *xs, *kvs, gain)
+        cost_estimate=estimate(heads, head_width, 0),
+    )(place, offsets, q_mine, *kvs)
 
 
 def sent_to_all(value, axes):
@@ -224,7 +272,7 @@
     normed = normed.reshape(-1, tokens)
     far = swapped(normed, "yl")
     near = swapped(normed, "core")
-    xs = (normed, near, far, swapped(far, "core"))
+    both = swapped(far, "core")
 
     half = along_z.shape[0] // 2
     top, bottom = along_z[:half], along_z[half:]
@@ -238,11 +286,18 @@
 
     gain = query_gain * (head_width ** (-0.5) * log2_e)
     gain = jnp.broadcast_to(gain[:, None], (head_width, head_width))
-    place = jnp.stack((part, chip, core, lax.axis_index("x"))).astype(jnp.int32)
     offsets = lax.dynamic_slice_in_dim(stick_offset * log2_e, member * heads, heads)
-    attended = attend(place, offsets, weights, xs, kvs, gain)
-    out = lax.all_to_all(attended, ("yl", "core"), split_axis=0, concat_axis=0, tiled=True)
-    return out.transpose(1, 0, 2).reshape(1, tokens, heads_all * head_width)
+    place = jnp.stack((part, core, lax.axis_index("x"), member, chip)).astype(jnp.int32)
+    xs = (far, both, normed, near)
+    theirs, q_mine = attend_first(place, offsets, weights, xs, kvs, gain)
+    arrived = swapped(theirs, "yl")
+    ours = attend_second(place, offsets, q_mine, kvs)
+    passed = swapped(jnp.stack((ours[1], arrived[1])), "core")
+    pairs = (ours[0], passed[0]), (arrived[0], passed[1])
+    (a, b), (c, d) = ((jnp.where(core == 0, p, q), jnp.where(core == 0, q, p)) for p, q in pairs)
+    flip = chip == 0
+    ordered = (jnp.where(flip, a, c), jnp.where(flip, b, d), jnp.where(flip, c, a), jnp.where(flip, d, b))
+    return jnp.concatenate(ordered, axis=1)[None]
 
 
 def solution(mesh):

time: 134 us -> 130 us (0.970)
  the two profiles are of different devices: /device:TPU:48 before, /device:TPU:57 now
where the time goes in v3:
time: 130 us; the launch traced here: 129 us
  starting transfers between devices  75.9 us (58%)
  waiting for transfers between devices  27 us (21%)
  Pallas kernels  16.9 us (13%)
  local copies, waits for them, and re-layouts  6.9 us (5%)
  other arithmetic  2.01 us (2%)
    ppermute x5, starting transfers between devices, swapped(): return lax.ppermute(value, axis, [(0, 1), (1, 0)])  28 us
    ppermute x6, starting transfers between devices, turned(): lax.ppermute(value, axis, [(i, (i + shift) % count) for i in range(count)])  20.6 us
    ppermute x3, waiting for transfers between devices, handed_on(): lax.ppermute(value, 'yh', [(i, i + shift) for i in range(count - shift)])  15.8 us
    all_to_all x1, starting transfers between devices, sent_to_all(): return lax.all_to_all(copies, axes, split_axis=0, concat_axis=0, tiled=True)  15 us
    pallas_call x1, Pallas kernels, attend_first(): pl.pallas_call(first_kernel, out_shape=(jax.ShapeDtypeStruct((cores, tile...  9.53 us
    ppermute x3, starting transfers between devices, flipped(): lax.ppermute(value, ('yl', 'core'), [(i, i ^ bits) for i in range(group)])  8.32 us
    pallas_call x1, Pallas kernels, attend_second(): pl.pallas_call(second_kernel, out_shape=jax.ShapeDtypeStruct((cores, tile...  7.34 us
    ppermute x6, waiting for transfers between devices, turned(): lax.ppermute(value, axis, [(i, (i + shift) % count) for i in range(count)])  5.81 us
  transfers between devices with their start and end apart: 18, of which 5 were waited for; matrix products, arithmetic and copies ran while one was open for 2% of the time, Pallas kernels for 6%

profile of v3, /device:TPU:57, one launch (start us, length us, event | category | flops | bytes accessed | tf_op | source)
XLA Modules:
  0.0 129.3 jit_solution(14871911291414441274)
XLA Ops:
  0.0 0.9 copy-done
  0.9 0.9 broadcast_in_dim.6
  1.8 15.0 %all-to-all-start = ((bf16[12,48,512]{2,1,0:T(8,128)(2,1)}), bf16[12,48,512]{2,1,0:T(8,128)(2,1)S(1)}, u32[]{:S(2)}, u32[]{:S(2)}) async-start(bf16[12,48,512]{2,1,0:T(8,128)(2,1)} %broadcast_in_dim.6), calls=%async_computation | async-start | bytes 1179648 | tf_op jit(solution)/shard_map/all_to_all | solution.py:216
  16.9 0.1 copy.23
  17.0 0.0 copy-start.7
  17.0 0.1 reshape.59
  17.1 0.2 multiply_reduce_fusion
  17.3 0.0 copy-start.9
  17.3 0.1 copy.24
  17.4 0.5 copy-done.7
  17.9 0.1 copy.26
  18.0 0.1 copy.27
  18.2 0.1 fusion.6
  18.4 2.9 %collective-permute-start.9 = (bf16[1,2,128,128]{3,2,1,0:T(8,128)(2,1)S(1)}, bf16[1,2,128,128]{3,2,1,0:T(8,128)(2,1)S(1)}, u32[]{:S(2)}, u32[]{:S(2)}) collective-permute-start(bf16[1,2,128,128]{3,2,1,0:T(8,128)(2,1)S(1)} %get-tuple-element.16), channel_id=1, source_target_pairs={{0,48},{48,0},{96,144},{144,96},{1,49},{49,1},{97,145},{145,97},{2... | collective-permute-start | bytes 196616 | tf_op jit(solution)/shard_map/ppermute | solution.py:229
  21.3 3.0 %collective-permute-start.10 = (bf16[1,2,128,128]{3,2,1,0:T(8,128)(2,1)S(1)}, bf16[1,2,128,128]{3,2,1,0:T(8,128)(2,1)S(1)}, u32[]{:S(2)}, u32[]{:S(2)}) collective-permute-start(bf16[1,2,128,128]{3,2,1,0:T(8,128)(2,1)S(1)} %get-tuple-element.17), channel_id=1, source_target_pairs={{0,96},{48,144},{96,0},{144,48},{1,97},{49,145},{97,1},{145,49},{2... | collective-permute-start | bytes 196616 | tf_op jit(solution)/shard_map/ppermute | solution.py:229
  24.2 2.5 %collective-permute-start.11 = (bf16[1,2,128,128]{3,2,1,0:T(8,128)(2,1)S(1)}, bf16[1,2,128,128]{3,2,1,0:T(8,128)(2,1)S(1)}, u32[]{:S(2)}, u32[]{:S(2)}) collective-permute-start(bf16[1,2,128,128]{3,2,1,0:T(8,128)(2,1)S(1)} %get-tuple-element.18), channel_id=1, source_target_pairs={{0,144},{48,96},{96,48},{144,0},{1,145},{49,97},{97,49},{145,1},{2... | collective-permute-start | bytes 196616 | tf_op jit(solution)/shard_map/ppermute | solution.py:229
  26.7 0.3 fusion
  27.0 0.3 fusion.3
  27.4 0.2 reshape.55
  27.6 0.1 pad.9.clone
  27.7 3.0 %collective-permute-start.6 = (bf16[2304,128]{1,0:T(8,128)(2,1)S(1)}, bf16[2304,128]{1,0:T(8,128)(2,1)S(1)}, u32[]{:S(2)}, u32[]{:S(2)}) collective-permute-start(bf16[2304,128]{1,0:T(8,128)(2,1)S(1)} %bitcast.41), channel_id=1, source_target_pairs={{0,96},{96,0},{1,97},{97,1},{2,98},{98,2},{3,99},{99,3},{4,100},{1... | collective-permute-start | bytes 1769480 | tf_op jit(solution)/shard_map/ppermute | solution.py:220
  30.7 2.4 %collective-permute-start.8 = (bf16[2304,128]{1,0:T(8,128)(2,1)S(1)}, bf16[2304,128]{1,0:T(8,128)(2,1)}, u32[]{:S(2)}, u32[]{:S(2)}) collective-permute-start(bf16[2304,128]{1,0:T(8,128)(2,1)S(1)} %bitcast.42), channel_id=1, source_target_pairs={{0,48},{48,0},{1,49},{49,1},{2,50},{50,2},{3,51},{51,3},{4,52},{52... | collective-permute-start | bytes 1769480 | tf_op jit(solution)/shard_map/ppermute | solution.py:220
  33.2 1.4 %collective-permute-start.14 = (bf16[4,2,128,128]{3,2,1,0:T(8,128)(2,1)S(1)}, bf16[4,2,128,128]{3,2,1,0:T(8,128)(2,1)}, u32[]{:S(2)}, u32[]{:S(2)}) collective-permute-start(bf16[4,2,128,128]{3,2,1,0:T(8,128)(2,1)S(1)} %pad_maximum_fusion.kv_own), channel_id=1, source_target_pairs={{0,576},{1,577},{2,578},{3,579},{4,580},{5,581},{6,582},{7,583},{8... | collective-permute-start | bytes 786440 | tf_op jit(solution)/shard_map/ppermute | solution.py:234
  34.6 1.3 collective-permute-start.13
  35.9 4.2 %all-to-all-done = bf16[12,48,512]{2,1,0:T(8,128)(2,1)S(1)} async-done(((bf16[12,48,512]{2,1,0:T(8,128)(2,1)}), bf16[12,48,512]{2,1,0:T(8,128)(2,1)S(1)}, u32[]{:S(2)}, u32[]{:S(2)}) %all-to-all-start) | async-done | bytes 589856 | tf_op jit(solution)/shard_map/all_to_all | solution.py:216
  40.2 0.8 copy-done.1
  41.0 3.1 %collective-permute-start = (bf16[288,512]{1,0:T(8,128)(2,1)S(1)}, bf16[288,512]{1,0:T(8,128)(2,1)S(1)}, u32[]{:S(2)}, u32[]{:S(2)}) collective-permute-start(bf16[288,512]{1,0:T(8,128)(2,1)S(1)} %bitcast.47), channel_id=1, source_target_pairs={{0,1},{1,2},{2,3},{3,0},{4,5},{5,6},{6,7},{7,4},{8,9},{9,10},{10,1... | collective-permute-start | bytes 884744 | tf_op jit(solution)/shard_map/ppermute | solution.py:225
  44.1 10.7 %collective-permute-done.14.kv_three = bf16[4,2,128,128]{3,2,1,0:T(8,128)(2,1)} collective-permute-done((bf16[4,2,128,128]{3,2,1,0:T(8,128)(2,1)S(1)}, bf16[4,2,128,128]{3,2,1,0:T(8,128)(2,1)}, u32[]{:S(2)}, u32[]{:S(2)}) %collective-permute-start.14) | collective-permute-done | bytes 262176 | tf_op jit(solution)/shard_map/ppermute | solution.py:234
  54.9 4.4 %collective-permute-start.3 = (bf16[288,512]{1,0:T(8,128)(2,1)S(1)}, bf16[288,512]{1,0:T(8,128)(2,1)}, u32[]{:S(2)}, u32[]{:S(2)}) collective-permute-start(bf16[288,512]{1,0:T(8,128)(2,1)S(1)} %bitcast.45), channel_id=1, source_target_pairs={{0,3},{1,0},{2,1},{3,2},{4,7},{5,4},{6,5},{7,6},{8,11},{9,8},{10,9... | collective-permute-start | bytes 884744 | tf_op jit(solution)/shard_map/ppermute | solution.py:225
  59.3 1.3 collective-permute-start.12
  60.6 4.0 %collective-permute-start.7 = (bf16[2304,128]{1,0:T(8,128)(2,1)S(1)}, bf16[2304,128]{1,0:T(8,128)(2,1)S(1)}, u32[]{:S(2)}, u32[]{:S(2)}) collective-permute-start(bf16[2304,128]{1,0:T(8,128)(2,1)S(1)} %collective-permute-done.6.x_far), channel_id=1, source_target_pairs={{0,48},{48,0},{1,49},{49,1},{2,50},{50,2},{3,51},{51,3},{4,52},{52... | collective-permute-start | bytes 1769480 | tf_op jit(solution)/shard_map/ppermute | solution.py:220
  64.6 5.1 %collective-permute-done.12.kv_one = bf16[4,2,128,128]{3,2,1,0:T(8,128)(2,1)S(1)} collective-permute-done((bf16[4,2,128,128]{3,2,1,0:T(8,128)(2,1)S(1)}, bf16[4,2,128,128]{3,2,1,0:T(8,128)(2,1)S(1)}, u32[]{:S(2)}, u32[]{:S(2)}) %collective-permute-start.12) | collective-permute-done | bytes 262176 | tf_op jit(solution)/shard_map/ppermute | solution.py:234
  69.7 4.7 %collective-permute-start.2 = (bf16[288,512]{1,0:T(8,128)(2,1)S(1)}, bf16[288,512]{1,0:T(8,128)(2,1)}, u32[]{:S(2)}, u32[]{:S(2)}) collective-permute-start(bf16[288,512]{1,0:T(8,128)(2,1)S(1)} %bitcast.48), channel_id=1, source_target_pairs={{0,3},{1,0},{2,1},{3,2},{4,7},{5,4},{6,5},{7,6},{8,11},{9,8},{10,9... | collective-permute-start | bytes 884744 | tf_op jit(solution)/shard_map/ppermute | solution.py:225
  74.4 1.9 %collective-permute-start.1 = (bf16[288,512]{1,0:T(8,128)(2,1)S(1)}, bf16[288,512]{1,0:T(8,128)(2,1)S(1)}, u32[]{:S(2)}, u32[]{:S(2)}) collective-permute-start(bf16[288,512]{1,0:T(8,128)(2,1)S(1)} %bitcast.46), channel_id=1, source_target_pairs={{0,1},{1,2},{2,3},{3,0},{4,5},{5,6},{6,7},{7,4},{8,9},{9,10},{10,1... | collective-permute-start | bytes 884744 | tf_op jit(solution)/shard_map/ppermute | solution.py:225
  76.4 2.1 %collective-permute-start.4 = (bf16[288,512]{1,0:T(8,128)(2,1)S(1)}, bf16[288,512]{1,0:T(8,128)(2,1)S(1)}, u32[]{:S(2)}, u32[]{:S(2)}) collective-permute-start(bf16[288,512]{1,0:T(8,128)(2,1)S(1)} %collective-permute-done.w_left), channel_id=1, source_target_pairs={{0,1},{1,2},{2,3},{3,0},{4,5},{5,6},{6,7},{7,4},{8,9},{9,10},{10,1... | collective-permute-start | bytes 884744 | tf_op jit(solution)/shard_map/ppermute | solution.py:225
  78.5 4.4 %collective-permute-start.5 = (bf16[288,512]{1,0:T(8,128)(2,1)}, bf16[288,512]{1,0:T(8,128)(2,1)}, u32[]{:S(2)}, u32[]{:S(2)}) collective-permute-start(bf16[288,512]{1,0:T(8,128)(2,1)} %collective-permute-done.3.w_right_end), channel_id=1, source_target_pairs={{0,3},{1,0},{2,1},{3,2},{4,7},{5,4},{6,5},{7,6},{8,11},{9,8},{10,9... | collective-permute-start | bytes 884744 | tf_op jit(solution)/shard_map/ppermute | solution.py:225
  82.9 0.7 dynamic_slice.19.offsets
  83.6 0.6 stack.35.place
  84.3 5.8 %collective-permute-done.4.w_far = bf16[288,512]{1,0:T(8,128)(2,1)S(1)} collective-permute-done((bf16[288,512]{1,0:T(8,128)(2,1)S(1)}, bf16[288,512]{1,0:T(8,128)(2,1)S(1)}, u32[]{:S(2)}, u32[]{:S(2)}) %collective-permute-start.4) | collective-permute-done | bytes 294944 | tf_op jit(solution)/shard_map/ppermute | solution.py:225
  90.1 0.7 broadcast_in_dim.7.gain
  90.8 9.5 %shard_map.82 = (bf16[2,128,512]{2,1,0:T(8,128)(2,1)}, bf16[4,128,256]{2,1,0:T(8,128)(2,1)}) custom-call(s32[5]{0:T(128)} %stack.35.place, f32[4]{0:T(128)} %dynamic_slice.19.offsets, bf16[576,512]{1,0:T(8,128)(2,1)} %bitcast.39, bf16[288,512]{1,0:T(8,128)(2,1)} %copy-done.12, bf16[288,512]{1,0:T(8,128)(2,1)} %copy-done.13, ...), custom_call_target="tpu_custom_call" | custom-call | flops 2281701376 | bytes 4194304 | tf_op jit(solution)/shard_map/pallas_call | solution.py:175
  100.4 14.5 %collective-permute-start.15 = (bf16[2,128,512]{2,1,0:T(8,128)(2,1)}, bf16[2,128,512]{2,1,0:T(8,128)(2,1)S(1)}, u32[]{:S(2)}, u32[]{:S(2)}) collective-permute-start(bf16[2,128,512]{2,1,0:T(8,128)(2,1)} %get-tuple-element.8), channel_id=1, source_target_pairs={{0,96},{96,0},{1,97},{97,1},{2,98},{98,2},{3,99},{99,3},{4,100},{1... | collective-permute-start | bytes 786440 | tf_op jit(solution)/shard_map/ppermute | solution.py:220
  114.9 7.3 %shard_map.83 = bf16[2,128,512]{2,1,0:T(8,128)(2,1)} custom-call(s32[5]{0:T(128)} %stack.35.place, f32[4]{0:T(128)} %dynamic_slice.19.offsets, bf16[4,128,256]{2,1,0:T(8,128)(2,1)} %get-tuple-element.7.q_rows, bf16[4,2,128,128]{3,2,1,0:T(8,128)(2,1)} %copy-done.5, bf16[4,2,128,128]{3,2,1,0:T(8,128)(2,1)} %copy-done.15, ...), custom_call_target="tpu_custom_call" | custom-call | flops 1073741824 | bytes 4194304 | tf_op jit(solution)/shard_map/pallas_call | solution.py:198
  122.3 0.0 slice-start
  122.3 0.9 slice-done
  123.2 4.1 %collective-permute-start.16 = (bf16[2,128,512]{2,1,0:T(8,128)(2,1)S(1)}, bf16[2,128,512]{2,1,0:T(8,128)(2,1)S(1)}, u32[]{:S(2)}, u32[]{:S(2)}) collective-permute-start(bf16[2,128,512]{2,1,0:T(8,128)(2,1)S(1)} %pad_maximum_fusion.1), channel_id=1, source_target_pairs={{0,48},{48,0},{1,49},{49,1},{2,50},{50,2},{3,51},{51,3},{4,52},{52... | collective-permute-start | bytes 786440 | tf_op jit(solution)/shard_map/ppermute | solution.py:220
  127.3 1.1 collective-permute-done.16
  128.5 0.8 maximum_bitcast_fusion
  (60 shorter events, 0.5 us)
Async XLA Ops:
  0.0 0.9 copy-start
  1.8 15.0 %copy-start.6 = (bf16[1,128,512]{2,1,0:T(8,128)(2,1)S(1)}, bf16[1,128,512]{2,1,0:T(8,128)(2,1)}, u32[]{:S(2)}) copy-start(bf16[1,128,512]{2,1,0:T(8,128)(2,1)} %param.12) | copy-start | bytes 393220
  1.8 38.4 %all-to-all-start = ((bf16[12,48,512]{2,1,0:T(8,128)(2,1)}), bf16[12,48,512]{2,1,0:T(8,128)(2,1)S(1)}, u32[]{:S(2)}, u32[]{:S(2)}) async-start(bf16[12,48,512]{2,1,0:T(8,128)(2,1)} %broadcast_in_dim.6), calls=%async_computation | async-start | bytes 1179648 | tf_op jit(solution)/shard_map/all_to_all | solution.py:216
  17.0 0.9 copy-start.7
  17.3 0.9 copy-start.9
  18.0 8.7 %copy-start.2 = (bf16[1,128,2064]{1,2,0:T(8,128)(2,1)S(1)}, bf16[1,128,2064]{1,2,0:T(8,128)(2,1)}, u32[]{:S(2)}) copy-start(bf16[1,128,2064]{1,2,0:T(8,128)(2,1)} %param.8) | copy-start | bytes 1585156
  18.3 8.7 %copy-start.8 = (f32[2064]{0:T(1024)S(1)}, f32[2064]{0:T(1024)}, u32[]{:S(2)}) copy-start(f32[2064]{0:T(1024)} %param.9) | copy-start | bytes 24772
  18.4 14.7 %collective-permute-start.9 = (bf16[1,2,128,128]{3,2,1,0:T(8,128)(2,1)S(1)}, bf16[1,2,128,128]{3,2,1,0:T(8,128)(2,1)S(1)}, u32[]{:S(2)}, u32[]{:S(2)}) collective-permute-start(bf16[1,2,128,128]{3,2,1,0:T(8,128)(2,1)S(1)} %get-tuple-element.16), channel_id=1, source_target_pairs={{0,48},{48,0},{96,144},{144,96},{1,49},{49,1},{97,145},{145,97},{2... | collective-permute-start | bytes 196616 | tf_op jit(solution)/shard_map/ppermute | solution.py:229
  21.3 11.9 %collective-permute-start.10 = (bf16[1,2,128,128]{3,2,1,0:T(8,128)(2,1)S(1)}, bf16[1,2,128,128]{3,2,1,0:T(8,128)(2,1)S(1)}, u32[]{:S(2)}, u32[]{:S(2)}) collective-permute-start(bf16[1,2,128,128]{3,2,1,0:T(8,128)(2,1)S(1)} %get-tuple-element.17), channel_id=1, source_target_pairs={{0,96},{48,144},{96,0},{144,48},{1,97},{49,145},{97,1},{145,49},{2... | collective-permute-start | bytes 196616 | tf_op jit(solution)/shard_map/ppermute | solution.py:229
  24.2 8.9 %collective-permute-start.11 = (bf16[1,2,128,128]{3,2,1,0:T(8,128)(2,1)S(1)}, bf16[1,2,128,128]{3,2,1,0:T(8,128)(2,1)S(1)}, u32[]{:S(2)}, u32[]{:S(2)}) collective-permute-start(bf16[1,2,128,128]{3,2,1,0:T(8,128)(2,1)S(1)} %get-tuple-element.18), channel_id=1, source_target_pairs={{0,144},{48,96},{96,48},{144,0},{1,145},{49,97},{97,49},{145,1},{2... | collective-permute-start | bytes 196616 | tf_op jit(solution)/shard_map/ppermute | solution.py:229
  27.7 12.5 %copy-start.3 = (bf16[4,12,48,128]{3,2,1,0:T(8,128)(2,1)}, bf16[4,12,48,128]{3,2,1,0:T(8,128)(2,1)S(1)}, u32[]{:S(2)}) copy-start(bf16[4,12,48,128]{3,2,1,0:T(8,128)(2,1)S(1)} %pad.9.clone) | copy-start | bytes 1769476
  27.7 32.9 %collective-permute-start.6 = (bf16[2304,128]{1,0:T(8,128)(2,1)S(1)}, bf16[2304,128]{1,0:T(8,128)(2,1)S(1)}, u32[]{:S(2)}, u32[]{:S(2)}) collective-permute-start(bf16[2304,128]{1,0:T(8,128)(2,1)S(1)} %bitcast.41), channel_id=1, source_target_pairs={{0,96},{96,0},{1,97},{97,1},{2,98},{98,2},{3,99},{99,3},{4,100},{1... | collective-permute-start | bytes 1769480 | tf_op jit(solution)/shard_map/ppermute | solution.py:220
  30.7 43.7 %collective-permute-start.8 = (bf16[2304,128]{1,0:T(8,128)(2,1)S(1)}, bf16[2304,128]{1,0:T(8,128)(2,1)}, u32[]{:S(2)}, u32[]{:S(2)}) collective-permute-start(bf16[2304,128]{1,0:T(8,128)(2,1)S(1)} %bitcast.42), channel_id=1, source_target_pairs={{0,48},{48,0},{1,49},{49,1},{2,50},{50,2},{3,51},{51,3},{4,52},{52... | collective-permute-start | bytes 1769480 | tf_op jit(solution)/shard_map/ppermute | solution.py:220
  33.2 26.1 %copy-start.5 = (bf16[4,2,128,128]{3,2,1,0:T(8,128)(2,1)}, bf16[4,2,128,128]{3,2,1,0:T(8,128)(2,1)S(1)}, u32[]{:S(2)}) copy-start(bf16[4,2,128,128]{3,2,1,0:T(8,128)(2,1)S(1)} %pad_maximum_fusion.kv_own) | copy-start | bytes 786436
  33.2 49.7 %copy-start.16 = (f32[16]{0:T(128)S(1)}, f32[16]{0:T(128)}, u32[]{:S(2)}) copy-start(f32[16]{0:T(128)} %param.15) | copy-start | bytes 196
  33.2 51.0 %copy-start.17 = (f32[128]{0:T(128)S(1)}, f32[128]{0:T(128)}, u32[]{:S(2)}) copy-start(f32[128]{0:T(128)} %param.11) | copy-start | bytes 1540
  33.2 21.6 %collective-permute-start.14 = (bf16[4,2,128,128]{3,2,1,0:T(8,128)(2,1)S(1)}, bf16[4,2,128,128]{3,2,1,0:T(8,128)(2,1)}, u32[]{:S(2)}, u32[]{:S(2)}) collective-permute-start(bf16[4,2,128,128]{3,2,1,0:T(8,128)(2,1)S(1)} %pad_maximum_fusion.kv_own), channel_id=1, source_target_pairs={{0,576},{1,577},{2,578},{3,579},{4,580},{5,581},{6,582},{7,583},{8... | collective-permute-start | bytes 786440 | tf_op jit(solution)/shard_map/ppermute | solution.py:234
  34.6 24.6 %collective-permute-start.13 = (bf16[4,2,128,128]{3,2,1,0:T(8,128)(2,1)S(1)}, bf16[4,2,128,128]{3,2,1,0:T(8,128)(2,1)}, u32[]{:S(2)}, u32[]{:S(2)}) collective-permute-start(bf16[4,2,128,128]{3,2,1,0:T(8,128)(2,1)S(1)} %pad_maximum_fusion.kv_own), channel_id=1, source_target_pairs={{0,384},{192,576},{1,385},{193,577},{2,386},{194,578},{3,387},{195... | collective-permute-start | bytes 786440 | tf_op jit(solution)/shard_map/ppermute | solution.py:234
  40.2 0.8 copy-start.1
  41.0 35.3 %collective-permute-start = (bf16[288,512]{1,0:T(8,128)(2,1)S(1)}, bf16[288,512]{1,0:T(8,128)(2,1)S(1)}, u32[]{:S(2)}, u32[]{:S(2)}) collective-permute-start(bf16[288,512]{1,0:T(8,128)(2,1)S(1)} %bitcast.47), channel_id=1, source_target_pairs={{0,1},{1,2},{2,3},{3,0},{4,5},{5,6},{6,7},{7,4},{8,9},{9,10},{10,1... | collective-permute-start | bytes 884744 | tf_op jit(solution)/shard_map/ppermute | solution.py:225
  54.9 23.6 %collective-permute-start.3 = (bf16[288,512]{1,0:T(8,128)(2,1)S(1)}, bf16[288,512]{1,0:T(8,128)(2,1)}, u32[]{:S(2)}, u32[]{:S(2)}) collective-permute-start(bf16[288,512]{1,0:T(8,128)(2,1)S(1)} %bitcast.45), channel_id=1, source_target_pairs={{0,3},{1,0},{2,1},{3,2},{4,7},{5,4},{6,5},{7,6},{8,11},{9,8},{10,9... | collective-permute-start | bytes 884744 | tf_op jit(solution)/shard_map/ppermute | solution.py:225
  59.3 10.4 %collective-permute-start.12 = (bf16[4,2,128,128]{3,2,1,0:T(8,128)(2,1)S(1)}, bf16[4,2,128,128]{3,2,1,0:T(8,128)(2,1)S(1)}, u32[]{:S(2)}, u32[]{:S(2)}) collective-permute-start(bf16[4,2,128,128]{3,2,1,0:T(8,128)(2,1)S(1)} %pad_maximum_fusion.kv_own), channel_id=1, source_target_pairs={{0,192},{192,384},{384,576},{1,193},{193,385},{385,577},{2,194},{1... | collective-permute-start | bytes 786440 | tf_op jit(solution)/shard_map/ppermute | solution.py:234
  60.6 30.2 %copy-start.10 = (bf16[2304,128]{1,0:T(8,128)(2,1)}, bf16[2304,128]{1,0:T(8,128)(2,1)S(1)}, u32[]{:S(2)}) copy-start(bf16[2304,128]{1,0:T(8,128)(2,1)S(1)} %collective-permute-done.6.x_far) | copy-start | bytes 1769476
  60.6 23.7 %collective-permute-start.7 = (bf16[2304,128]{1,0:T(8,128)(2,1)S(1)}, bf16[2304,128]{1,0:T(8,128)(2,1)S(1)}, u32[]{:S(2)}, u32[]{:S(2)}) collective-permute-start(bf16[2304,128]{1,0:T(8,128)(2,1)S(1)} %collective-permute-done.6.x_far), channel_id=1, source_target_pairs={{0,48},{48,0},{1,49},{49,1},{2,50},{50,2},{3,51},{51,3},{4,52},{52... | collective-permute-start | bytes 1769480 | tf_op jit(solution)/shard_map/ppermute | solution.py:220
  69.7 8.8 %copy-start.15 = (bf16[4,2,128,128]{3,2,1,0:T(8,128)(2,1)}, bf16[4,2,128,128]{3,2,1,0:T(8,128)(2,1)S(1)}, u32[]{:S(2)}) copy-start(bf16[4,2,128,128]{3,2,1,0:T(8,128)(2,1)S(1)} %collective-permute-done.12.kv_one) | copy-start | bytes 786436
  69.7 14.5 %collective-permute-start.2 = (bf16[288,512]{1,0:T(8,128)(2,1)S(1)}, bf16[288,512]{1,0:T(8,128)(2,1)}, u32[]{:S(2)}, u32[]{:S(2)}) collective-permute-start(bf16[288,512]{1,0:T(8,128)(2,1)S(1)} %bitcast.48), channel_id=1, source_target_pairs={{0,3},{1,0},{2,1},{3,2},{4,7},{5,4},{6,5},{7,6},{8,11},{9,8},{10,9... | collective-permute-start | bytes 884744 | tf_op jit(solution)/shard_map/ppermute | solution.py:225
  74.4 9.9 %collective-permute-start.1 = (bf16[288,512]{1,0:T(8,128)(2,1)S(1)}, bf16[288,512]{1,0:T(8,128)(2,1)S(1)}, u32[]{:S(2)}, u32[]{:S(2)}) collective-permute-start(bf16[288,512]{1,0:T(8,128)(2,1)S(1)} %bitcast.46), channel_id=1, source_target_pairs={{0,1},{1,2},{2,3},{3,0},{4,5},{5,6},{6,7},{7,4},{8,9},{9,10},{10,1... | collective-permute-start | bytes 884744 | tf_op jit(solution)/shard_map/ppermute | solution.py:225
  76.3 14.5 %copy-start.12 = (bf16[288,512]{1,0:T(8,128)(2,1)}, bf16[288,512]{1,0:T(8,128)(2,1)S(1)}, u32[]{:S(2)}) copy-start(bf16[288,512]{1,0:T(8,128)(2,1)S(1)} %collective-permute-done.w_left) | copy-start | bytes 884740
  76.4 13.7 %collective-permute-start.4 = (bf16[288,512]{1,0:T(8,128)(2,1)S(1)}, bf16[288,512]{1,0:T(8,128)(2,1)S(1)}, u32[]{:S(2)}, u32[]{:S(2)}) collective-permute-start(bf16[288,512]{1,0:T(8,128)(2,1)S(1)} %collective-permute-done.w_left), channel_id=1, source_target_pairs={{0,1},{1,2},{2,3},{3,0},{4,5},{5,6},{6,7},{7,4},{8,9},{9,10},{10,1... | collective-permute-start | bytes 884744 | tf_op jit(solution)/shard_map/ppermute | solution.py:225
  78.5 11.6 %collective-permute-start.5 = (bf16[288,512]{1,0:T(8,128)(2,1)}, bf16[288,512]{1,0:T(8,128)(2,1)}, u32[]{:S(2)}, u32[]{:S(2)}) collective-permute-start(bf16[288,512]{1,0:T(8,128)(2,1)} %collective-permute-done.3.w_right_end), channel_id=1, source_target_pairs={{0,3},{1,0},{2,1},{3,2},{4,7},{5,4},{6,5},{7,6},{8,11},{9,8},{10,9... | collective-permute-start | bytes 884744 | tf_op jit(solution)/shard_map/ppermute | solution.py:225
  84.2 6.6 %copy-start.11 = (bf16[2304,128]{1,0:T(8,128)(2,1)}, bf16[2304,128]{1,0:T(8,128)(2,1)S(1)}, u32[]{:S(2)}) copy-start(bf16[2304,128]{1,0:T(8,128)(2,1)S(1)} %collective-permute-done.7.x_both) | copy-start | bytes 1769476
  84.3 6.6 %copy-start.13 = (bf16[288,512]{1,0:T(8,128)(2,1)}, bf16[288,512]{1,0:T(8,128)(2,1)S(1)}, u32[]{:S(2)}) copy-start(bf16[288,512]{1,0:T(8,128)(2,1)S(1)} %collective-permute-done.1.w_left_end) | copy-start | bytes 884740
  90.1 0.8 copy-start.14
  100.4 21.9 %collective-permute-start.15 = (bf16[2,128,512]{2,1,0:T(8,128)(2,1)}, bf16[2,128,512]{2,1,0:T(8,128)(2,1)S(1)}, u32[]{:S(2)}, u32[]{:S(2)}) collective-permute-start(bf16[2,128,512]{2,1,0:T(8,128)(2,1)} %get-tuple-element.8), channel_id=1, source_target_pairs={{0,96},{96,0},{1,97},{97,1},{2,98},{98,2},{3,99},{99,3},{4,100},{1... | collective-permute-start | bytes 786440 | tf_op jit(solution)/shard_map/ppermute | solution.py:220
  122.3 0.9 slice-start
  122.3 6.1 %copy-start.4 = (bf16[2,128,512]{2,1,0:T(8,128)(2,1)S(1)}, bf16[2,128,512]{2,1,0:T(8,128)(2,1)}, u32[]{:S(2)}) copy-start(bf16[2,128,512]{2,1,0:T(8,128)(2,1)} %shard_map.83) | copy-start | bytes 786436
  123.2 5.2 %collective-permute-start.16 = (bf16[2,128,512]{2,1,0:T(8,128)(2,1)S(1)}, bf16[2,128,512]{2,1,0:T(8,128)(2,1)S(1)}, u32[]{:S(2)}, u32[]{:S(2)}) collective-permute-start(bf16[2,128,512]{2,1,0:T(8,128)(2,1)S(1)} %pad_maximum_fusion.1), channel_id=1, source_target_pairs={{0,48},{48,0},{1,49},{49,1},{2,50},{50,2},{3,51},{51,3},{4,52},{52... | collective-permute-start | bytes 786440 | tf_op jit(solution)/shard_map/ppermute | solution.py:220

commit v4 on v2

--- a/solution.py
+++ b/solution.py
@@ -47,10 +47,11 @@
 
 def attend_kernel(
     place, offsets, w_own, w_left, w_left_end, w_right, w_right_end, w_far, w_far_end, x_own, x_core, x_far, x_both,
-    kv_own, kv_one, kv_two, kv_three, gain, out, q_rows, total, carries,
+    kv_own, kv_one, kv_two, kv_three, gain, out_own, out_core, out_far, out_both, q_rows, total, carries,
 ):
     part, chip, core, column = place[0], place[1], place[2], place[3]
     member = chip * cores + core
+    outs = (out_own, out_core, out_far, out_both)
     head_width = gain.shape[0]
     heads = offsets.shape[0]
     span = w_own.shape[0]
@@ -133,12 +134,12 @@
                     carries[h, t] = carry
 
     for h in range(heads):
+        lanes = slice(h * head_width, (h + 1) * head_width)
         for t in range(2):
-            rows = total[h, t].T.astype(jnp.bfloat16)
-            for c in range(2):
-                out[2 * t + c, :, h * head_width : (h + 1) * head_width] = rows[
-                    c * half : (c + 1) * half
-                ]
+            rows = total[h, jnp.bitwise_xor(chip, t)].T.astype(jnp.bfloat16)
+            low, high = rows[: tile // 2], rows[tile // 2 :]
+            outs[2 * t][:, lanes] = jnp.where(core == 0, low, high)
+            outs[2 * t + 1][:, lanes] = jnp.where(core == 0, high, low)
 
 
 def attend(place, offsets, weights, xs, kvs, gain):
@@ -150,9 +151,9 @@
     flops += heads * 8 * 2 * tile * tile * (2 * head_width + tile)
     return pl.pallas_call(
         attend_kernel,
-        out_shape=jax.ShapeDtypeStruct((group, tile // 2, heads * head_width), jnp.bfloat16),
+        out_shape=[jax.ShapeDtypeStruct((tile // 2, heads * head_width), jnp.bfloat16)] * group,
         in_specs=[smem, smem, *[vmem] * 16],
-        out_specs=vmem,
+        out_specs=[vmem] * group,
         scratch_shapes=[
             pltpu.VMEM((2, heads, head_width, tile), jnp.bfloat16),
             pltpu.VMEM((heads, 2, head_width, tile), jnp.float32),
@@ -241,8 +242,14 @@
     place = jnp.stack((part, chip, core, lax.axis_index("x"))).astype(jnp.int32)
     offsets = lax.dynamic_slice_in_dim(stick_offset * log2_e, member * heads, heads)
     attended = attend(place, offsets, weights, xs, kvs, gain)
-    out = lax.all_to_all(attended, ("yl", "core"), split_axis=0, concat_axis=0, tiled=True)
-    return out.transpose(1, 0, 2).reshape(1, tokens, heads_all * head_width)
+    third = flipped(attended[2], 2)
+    fourth = flipped(attended[3], 3)
+    second = flipped(attended[1], 1)
+    pairs = (attended[0], second), (third, fourth)
+    (a, b), (c, d) = ((jnp.where(core == 0, p, q), jnp.where(core == 0, q, p)) for p, q in pairs)
+    flip = chip == 0
+    ordered = (jnp.where(flip, a, c), jnp.where(flip, b, d), jnp.where(flip, c, a), jnp.where(flip, d, b))
+    return jnp.concatenate(ordered, axis=1)[None]
 
 
 def solution(mesh):

time: 134 us -> 135 us (level)
  the two profiles are of different devices: /device:TPU:48 before, /device:TPU:57 now
where the time goes in v4:
time: 135 us; the launch traced here: 134 us
  starting transfers between devices  77.6 us (57%)
  waiting for transfers between devices  33.7 us (25%)
  Pallas kernels  13 us (10%)
  local copies, waits for them, and re-layouts  5.46 us (4%)
  other arithmetic  3.52 us (3%)
    ppermute x6, starting transfers between devices, flipped(): lax.ppermute(value, ('yl', 'core'), [(i, i ^ bits) for i in range(group)])  29.7 us
    ppermute x6, starting transfers between devices, turned(): lax.ppermute(value, axis, [(i, (i + shift) % count) for i in range(count)])  20.3 us
    ppermute x3, waiting for transfers between devices, handed_on(): lax.ppermute(value, 'yh', [(i, i + shift) for i in range(count - shift)])  16.6 us
    all_to_all x1, starting transfers between devices, sent_to_all(): return lax.all_to_all(copies, axes, split_axis=0, concat_axis=0, tiled=True)  15 us
    pallas_call x1, Pallas kernels, attend(): pl.pallas_call(attend_kernel, out_shape=[jax.ShapeDtypeStruct((tile // 2,...  13 us
    ppermute x6, waiting for transfers between devices, flipped(): lax.ppermute(value, ('yl', 'core'), [(i, i ^ bits) for i in range(group)])  10 us
    ppermute x3, starting transfers between devices, swapped(): return lax.ppermute(value, axis, [(0, 1), (1, 0)])  8.65 us
    ppermute x6, waiting for transfers between devices, turned(): lax.ppermute(value, axis, [(i, (i + shift) % count) for i in range(count)])  7.08 us
  transfers between devices with their start and end apart: 19, of which 8 were waited for; matrix products, arithmetic and copies ran while one was open for 2% of the time, Pallas kernels for 0%

profile of v4, /device:TPU:57, one launch (start us, length us, event | category | flops | bytes accessed | tf_op | source)
XLA Modules:
  0.0 133.9 jit_solution(2108865328385420120)
XLA Ops:
  0.0 0.9 copy-done
  0.9 0.9 broadcast_in_dim.6
  1.8 15.0 %all-to-all-start = ((bf16[12,48,512]{2,1,0:T(8,128)(2,1)}), bf16[12,48,512]{2,1,0:T(8,128)(2,1)S(1)}, u32[]{:S(2)}, u32[]{:S(2)}) async-start(bf16[12,48,512]{2,1,0:T(8,128)(2,1)} %broadcast_in_dim.6), calls=%async_computation | async-start | bytes 1179648 | tf_op jit(solution)/shard_map/all_to_all | solution.py:169
  16.9 0.3 fusion
  17.2 0.3 fusion.3
  17.5 0.2 reshape.39
  17.8 0.1 pad.9.clone
  17.8 3.0 %collective-permute-start.7 = (bf16[2304,128]{1,0:T(8,128)(2,1)S(1)}, bf16[2304,128]{1,0:T(8,128)(2,1)S(1)}, u32[]{:S(2)}, u32[]{:S(2)}) collective-permute-start(bf16[2304,128]{1,0:T(8,128)(2,1)S(1)} %bitcast.32), channel_id=1, source_target_pairs={{0,96},{96,0},{1,97},{97,1},{2,98},{98,2},{3,99},{99,3},{4,100},{1... | collective-permute-start | bytes 1769480 | tf_op jit(solution)/shard_map/ppermute | solution.py:173
  20.8 0.1 copy.23
  21.0 0.1 reshape.43
  21.1 0.2 multiply_reduce_fusion
  21.3 0.1 copy.24
  21.4 0.5 copy-done.6
  21.8 0.1 copy.26
  22.0 0.1 copy.27
  22.2 0.1 fusion.6
  22.3 3.1 %collective-permute-start.9 = (bf16[1,2,128,128]{3,2,1,0:T(8,128)(2,1)S(1)}, bf16[1,2,128,128]{3,2,1,0:T(8,128)(2,1)S(1)}, u32[]{:S(2)}, u32[]{:S(2)}) collective-permute-start(bf16[1,2,128,128]{3,2,1,0:T(8,128)(2,1)S(1)} %get-tuple-element.20), channel_id=1, source_target_pairs={{0,48},{48,0},{96,144},{144,96},{1,49},{49,1},{97,145},{145,97},{2... | collective-permute-start | bytes 196616 | tf_op jit(solution)/shard_map/ppermute | solution.py:182
  25.5 2.3 %collective-permute-start.10 = (bf16[1,2,128,128]{3,2,1,0:T(8,128)(2,1)S(1)}, bf16[1,2,128,128]{3,2,1,0:T(8,128)(2,1)S(1)}, u32[]{:S(2)}, u32[]{:S(2)}) collective-permute-start(bf16[1,2,128,128]{3,2,1,0:T(8,128)(2,1)S(1)} %get-tuple-element.21), channel_id=1, source_target_pairs={{0,96},{48,144},{96,0},{144,48},{1,97},{49,145},{97,1},{145,49},{2... | collective-permute-start | bytes 196616 | tf_op jit(solution)/shard_map/ppermute | solution.py:182
  27.8 3.2 %collective-permute-start.11 = (bf16[1,2,128,128]{3,2,1,0:T(8,128)(2,1)S(1)}, bf16[1,2,128,128]{3,2,1,0:T(8,128)(2,1)S(1)}, u32[]{:S(2)}, u32[]{:S(2)}) collective-permute-start(bf16[1,2,128,128]{3,2,1,0:T(8,128)(2,1)S(1)} %get-tuple-element.22), channel_id=1, source_target_pairs={{0,144},{48,96},{96,48},{144,0},{1,145},{49,97},{97,49},{145,1},{2... | collective-permute-start | bytes 196616 | tf_op jit(solution)/shard_map/ppermute | solution.py:182
  31.0 2.1 %collective-permute-start.6 = (bf16[2304,128]{1,0:T(8,128)(2,1)S(1)}, bf16[2304,128]{1,0:T(8,128)(2,1)}, u32[]{:S(2)}, u32[]{:S(2)}) collective-permute-start(bf16[2304,128]{1,0:T(8,128)(2,1)S(1)} %bitcast.33), channel_id=1, source_target_pairs={{0,48},{48,0},{1,49},{49,1},{2,50},{50,2},{3,51},{51,3},{4,52},{52... | collective-permute-start | bytes 1769480 | tf_op jit(solution)/shard_map/ppermute | solution.py:173
  33.1 1.9 %collective-permute-done.10 = bf16[1,2,128,128]{3,2,1,0:T(8,128)(2,1)S(1)} collective-permute-done((bf16[1,2,128,128]{3,2,1,0:T(8,128)(2,1)S(1)}, bf16[1,2,128,128]{3,2,1,0:T(8,128)(2,1)S(1)}, u32[]{:S(2)}, u32[]{:S(2)}) %collective-permute-start.10) | collective-permute-done | bytes 65568 | tf_op jit(solution)/shard_map/ppermute | solution.py:182
  35.1 2.5 %collective-permute-done.11 = bf16[1,2,128,128]{3,2,1,0:T(8,128)(2,1)S(1)} collective-permute-done((bf16[1,2,128,128]{3,2,1,0:T(8,128)(2,1)S(1)}, bf16[1,2,128,128]{3,2,1,0:T(8,128)(2,1)S(1)}, u32[]{:S(2)}, u32[]{:S(2)}) %collective-permute-start.11) | collective-permute-done | bytes 65568 | tf_op jit(solution)/shard_map/ppermute | solution.py:182
  37.7 1.4 %collective-permute-start.14 = (bf16[4,2,128,128]{3,2,1,0:T(8,128)(2,1)S(1)}, bf16[4,2,128,128]{3,2,1,0:T(8,128)(2,1)S(1)}, u32[]{:S(2)}, u32[]{:S(2)}) collective-permute-start(bf16[4,2,128,128]{3,2,1,0:T(8,128)(2,1)S(1)} %pad_maximum_fusion.kv_own), channel_id=1, source_target_pairs={{0,576},{1,577},{2,578},{3,579},{4,580},{5,581},{6,582},{7,583},{8... | collective-permute-start | bytes 786440 | tf_op jit(solution)/shard_map/ppermute | solution.py:187
  39.1 1.3 collective-permute-start.13
  40.5 0.8 copy-done.1
  41.2 3.1 %collective-permute-start = (bf16[288,512]{1,0:T(8,128)(2,1)S(1)}, bf16[288,512]{1,0:T(8,128)(2,1)S(1)}, u32[]{:S(2)}, u32[]{:S(2)}) collective-permute-start(bf16[288,512]{1,0:T(8,128)(2,1)S(1)} %bitcast.38), channel_id=1, source_target_pairs={{0,1},{1,2},{2,3},{3,0},{4,5},{5,6},{6,7},{7,4},{8,9},{9,10},{10,1... | collective-permute-start | bytes 884744 | tf_op jit(solution)/shard_map/ppermute | solution.py:178
  44.4 11.0 %collective-permute-done.14.kv_three = bf16[4,2,128,128]{3,2,1,0:T(8,128)(2,1)S(1)} collective-permute-done((bf16[4,2,128,128]{3,2,1,0:T(8,128)(2,1)S(1)}, bf16[4,2,128,128]{3,2,1,0:T(8,128)(2,1)S(1)}, u32[]{:S(2)}, u32[]{:S(2)}) %collective-permute-start.14) | collective-permute-done | bytes 262176 | tf_op jit(solution)/shard_map/ppermute | solution.py:187
  55.3 4.4 %collective-permute-start.3 = (bf16[288,512]{1,0:T(8,128)(2,1)S(1)}, bf16[288,512]{1,0:T(8,128)(2,1)}, u32[]{:S(2)}, u32[]{:S(2)}) collective-permute-start(bf16[288,512]{1,0:T(8,128)(2,1)S(1)} %bitcast.36), channel_id=1, source_target_pairs={{0,3},{1,0},{2,1},{3,2},{4,7},{5,4},{6,5},{7,6},{8,11},{9,8},{10,9... | collective-permute-start | bytes 884744 | tf_op jit(solution)/shard_map/ppermute | solution.py:178
  59.7 1.3 collective-permute-start.12
  61.1 3.5 %collective-permute-start.8 = (bf16[2304,128]{1,0:T(8,128)(2,1)S(1)}, bf16[2304,128]{1,0:T(8,128)(2,1)S(1)}, u32[]{:S(2)}, u32[]{:S(2)}) collective-permute-start(bf16[2304,128]{1,0:T(8,128)(2,1)S(1)} %collective-permute-done.7.x_far), channel_id=1, source_target_pairs={{0,48},{48,0},{1,49},{49,1},{2,50},{50,2},{3,51},{51,3},{4,52},{52... | collective-permute-start | bytes 1769480 | tf_op jit(solution)/shard_map/ppermute | solution.py:173
  64.6 0.7 dynamic_slice.19.offsets
  65.3 5.6 %collective-permute-done.12.kv_one = bf16[4,2,128,128]{3,2,1,0:T(8,128)(2,1)} collective-permute-done((bf16[4,2,128,128]{3,2,1,0:T(8,128)(2,1)S(1)}, bf16[4,2,128,128]{3,2,1,0:T(8,128)(2,1)}, u32[]{:S(2)}, u32[]{:S(2)}) %collective-permute-start.12) | collective-permute-done | bytes 262176 | tf_op jit(solution)/shard_map/ppermute | solution.py:187
  70.9 4.4 %collective-permute-start.2 = (bf16[288,512]{1,0:T(8,128)(2,1)S(1)}, bf16[288,512]{1,0:T(8,128)(2,1)S(1)}, u32[]{:S(2)}, u32[]{:S(2)}) collective-permute-start(bf16[288,512]{1,0:T(8,128)(2,1)S(1)} %bitcast.39), channel_id=1, source_target_pairs={{0,3},{1,0},{2,1},{3,2},{4,7},{5,4},{6,5},{7,6},{8,11},{9,8},{10,9... | collective-permute-start | bytes 884744 | tf_op jit(solution)/shard_map/ppermute | solution.py:178
  75.3 1.9 %collective-permute-start.1 = (bf16[288,512]{1,0:T(8,128)(2,1)S(1)}, bf16[288,512]{1,0:T(8,128)(2,1)S(1)}, u32[]{:S(2)}, u32[]{:S(2)}) collective-permute-start(bf16[288,512]{1,0:T(8,128)(2,1)S(1)} %bitcast.37), channel_id=1, source_target_pairs={{0,1},{1,2},{2,3},{3,0},{4,5},{5,6},{6,7},{7,4},{8,9},{9,10},{10,1... | collective-permute-start | bytes 884744 | tf_op jit(solution)/shard_map/ppermute | solution.py:178
  77.3 2.1 %collective-permute-start.4 = (bf16[288,512]{1,0:T(8,128)(2,1)S(1)}, bf16[288,512]{1,0:T(8,128)(2,1)S(1)}, u32[]{:S(2)}, u32[]{:S(2)}) collective-permute-start(bf16[288,512]{1,0:T(8,128)(2,1)S(1)} %collective-permute-done.w_left), channel_id=1, source_target_pairs={{0,1},{1,2},{2,3},{3,0},{4,5},{5,6},{6,7},{7,4},{8,9},{9,10},{10,1... | collective-permute-start | bytes 884744 | tf_op jit(solution)/shard_map/ppermute | solution.py:178
  79.4 4.4 %collective-permute-start.5 = (bf16[288,512]{1,0:T(8,128)(2,1)}, bf16[288,512]{1,0:T(8,128)(2,1)S(1)}, u32[]{:S(2)}, u32[]{:S(2)}) collective-permute-start(bf16[288,512]{1,0:T(8,128)(2,1)} %collective-permute-done.3.w_right_end), channel_id=1, source_target_pairs={{0,3},{1,0},{2,1},{3,2},{4,7},{5,4},{6,5},{7,6},{8,11},{9,8},{10,9... | collective-permute-start | bytes 884744 | tf_op jit(solution)/shard_map/ppermute | solution.py:178
  83.8 0.6 pad_add_fusion.place
  84.5 0.8 collective-permute-done.1.w_left_end
  85.2 6.3 %collective-permute-done.4.w_far = bf16[288,512]{1,0:T(8,128)(2,1)S(1)} collective-permute-done((bf16[288,512]{1,0:T(8,128)(2,1)S(1)}, bf16[288,512]{1,0:T(8,128)(2,1)S(1)}, u32[]{:S(2)}, u32[]{:S(2)}) %collective-permute-start.4) | collective-permute-done | bytes 294944 | tf_op jit(solution)/shard_map/ppermute | solution.py:178
  91.6 0.8 broadcast_in_dim.7.gain
  92.4 13.0 %shard_map.82 = (bf16[128,512]{1,0:T(8,128)(2,1)}, bf16[128,512]{1,0:T(8,128)(2,1)}, bf16[128,512]{1,0:T(8,128)(2,1)}, bf16[128,512]{1,0:T(8,128)(2,1)}) custom-call(s32[4]{0:T(128)} %pad_add_fusion.place, f32[4]{0:T(128)} %dynamic_slice.19.offsets, bf16[576,512]{1,0:T(8,128)(2,1)} %bitcast.30, bf16[288,512]{1,0:T(8,128)(2,1)} %copy-done.11, ...), custom_call_target="tpu_custom_call" | custom-call | flops 3355443200 | bytes 4194304 | tf_op jit(solution)/shard_map/pallas_call | solution.py:152
  105.4 4.5 %collective-permute-start.15 = (bf16[128,512]{1,0:T(8,128)(2,1)}, bf16[128,512]{1,0:T(8,128)(2,1)S(1)}, u32[]{:S(2)}, u32[]{:S(2)}) collective-permute-start(bf16[128,512]{1,0:T(8,128)(2,1)} %get-tuple-element.10), channel_id=1, source_target_pairs={{0,48},{48,0},{96,144},{144,96},{1,49},{49,1},{97,145},{145,97},{2... | collective-permute-start | bytes 393224 | tf_op jit(solution)/shard_map/ppermute | solution.py:182
  110.0 14.6 %collective-permute-start.16 = (bf16[128,512]{1,0:T(8,128)(2,1)}, bf16[128,512]{1,0:T(8,128)(2,1)S(1)}, u32[]{:S(2)}, u32[]{:S(2)}) collective-permute-start(bf16[128,512]{1,0:T(8,128)(2,1)} %get-tuple-element.11), channel_id=1, source_target_pairs={{0,96},{48,144},{96,0},{144,48},{1,97},{49,145},{97,1},{145,49},{2... | collective-permute-start | bytes 393224 | tf_op jit(solution)/shard_map/ppermute | solution.py:182
  124.6 1.9 %collective-permute-start.17 = (bf16[128,512]{1,0:T(8,128)(2,1)}, bf16[128,512]{1,0:T(8,128)(2,1)S(1)}, u32[]{:S(2)}, u32[]{:S(2)}) collective-permute-start(bf16[128,512]{1,0:T(8,128)(2,1)} %get-tuple-element.12), channel_id=1, source_target_pairs={{0,144},{48,96},{96,48},{144,0},{1,145},{49,97},{97,49},{145,1},{2... | collective-permute-start | bytes 393224 | tf_op jit(solution)/shard_map/ppermute | solution.py:182
  126.6 2.1 %collective-permute-done.16 = bf16[128,512]{1,0:T(8,128)(2,1)S(1)} collective-permute-done((bf16[128,512]{1,0:T(8,128)(2,1)}, bf16[128,512]{1,0:T(8,128)(2,1)S(1)}, u32[]{:S(2)}, u32[]{:S(2)}) %collective-permute-start.16) | collective-permute-done | bytes 131104 | tf_op jit(solution)/shard_map/ppermute | solution.py:182
  128.7 3.4 %collective-permute-done.17 = bf16[128,512]{1,0:T(8,128)(2,1)S(1)} collective-permute-done((bf16[128,512]{1,0:T(8,128)(2,1)}, bf16[128,512]{1,0:T(8,128)(2,1)S(1)}, u32[]{:S(2)}, u32[]{:S(2)}) %collective-permute-start.17) | collective-permute-done | bytes 131104 | tf_op jit(solution)/shard_map/ppermute | solution.py:182
  132.1 1.0 broadcast_select_fusion.7
  133.1 0.8 maximum_bitcast_fusion
  (59 shorter events, 0.4 us)
Async XLA Ops:
  0.0 0.9 copy-start
  1.8 15.0 %copy-start.2 = (bf16[1,128,2064]{1,2,0:T(8,128)(2,1)S(1)}, bf16[1,128,2064]{1,2,0:T(8,128)(2,1)}, u32[]{:S(2)}) copy-start(bf16[1,128,2064]{1,2,0:T(8,128)(2,1)} %param.8) | copy-start | bytes 1585156
  1.8 15.3 %copy-start.7 = (f32[2064]{0:T(1024)S(1)}, f32[2064]{0:T(1024)}, u32[]{:S(2)}) copy-start(f32[2064]{0:T(1024)} %param.9) | copy-start | bytes 24772
  1.8 38.6 %all-to-all-start = ((bf16[12,48,512]{2,1,0:T(8,128)(2,1)}), bf16[12,48,512]{2,1,0:T(8,128)(2,1)S(1)}, u32[]{:S(2)}, u32[]{:S(2)}) async-start(bf16[12,48,512]{2,1,0:T(8,128)(2,1)} %broadcast_in_dim.6), calls=%async_computation | async-start | bytes 1179648 | tf_op jit(solution)/shard_map/all_to_all | solution.py:169
  17.7 3.1 %copy-start.5 = (bf16[1,128,512]{2,1,0:T(8,128)(2,1)S(1)}, bf16[1,128,512]{2,1,0:T(8,128)(2,1)}, u32[]{:S(2)}) copy-start(bf16[1,128,512]{2,1,0:T(8,128)(2,1)} %param.12) | copy-start | bytes 393220
  17.8 13.1 %copy-start.3 = (bf16[4,12,48,128]{3,2,1,0:T(8,128)(2,1)}, bf16[4,12,48,128]{3,2,1,0:T(8,128)(2,1)S(1)}, u32[]{:S(2)}) copy-start(bf16[4,12,48,128]{3,2,1,0:T(8,128)(2,1)S(1)} %pad.9.clone) | copy-start | bytes 1769476
  17.8 43.2 %collective-permute-start.7 = (bf16[2304,128]{1,0:T(8,128)(2,1)S(1)}, bf16[2304,128]{1,0:T(8,128)(2,1)S(1)}, u32[]{:S(2)}, u32[]{:S(2)}) collective-permute-start(bf16[2304,128]{1,0:T(8,128)(2,1)S(1)} %bitcast.32), channel_id=1, source_target_pairs={{0,96},{96,0},{1,97},{97,1},{2,98},{98,2},{3,99},{99,3},{4,100},{1... | collective-permute-start | bytes 1769480 | tf_op jit(solution)/shard_map/ppermute | solution.py:173
  20.9 0.9 copy-start.6
  21.3 0.9 copy-start.8
  22.3 10.8 %collective-permute-start.9 = (bf16[1,2,128,128]{3,2,1,0:T(8,128)(2,1)S(1)}, bf16[1,2,128,128]{3,2,1,0:T(8,128)(2,1)S(1)}, u32[]{:S(2)}, u32[]{:S(2)}) collective-permute-start(bf16[1,2,128,128]{3,2,1,0:T(8,128)(2,1)S(1)} %get-tuple-element.20), channel_id=1, source_target_pairs={{0,48},{48,0},{96,144},{144,96},{1,49},{49,1},{97,145},{145,97},{2... | collective-permute-start | bytes 196616 | tf_op jit(solution)/shard_map/ppermute | solution.py:182
  25.5 9.6 %collective-permute-start.10 = (bf16[1,2,128,128]{3,2,1,0:T(8,128)(2,1)S(1)}, bf16[1,2,128,128]{3,2,1,0:T(8,128)(2,1)S(1)}, u32[]{:S(2)}, u32[]{:S(2)}) collective-permute-start(bf16[1,2,128,128]{3,2,1,0:T(8,128)(2,1)S(1)} %get-tuple-element.21), channel_id=1, source_target_pairs={{0,96},{48,144},{96,0},{144,48},{1,97},{49,145},{97,1},{145,49},{2... | collective-permute-start | bytes 196616 | tf_op jit(solution)/shard_map/ppermute | solution.py:182
  27.8 9.8 %collective-permute-start.11 = (bf16[1,2,128,128]{3,2,1,0:T(8,128)(2,1)S(1)}, bf16[1,2,128,128]{3,2,1,0:T(8,128)(2,1)S(1)}, u32[]{:S(2)}, u32[]{:S(2)}) collective-permute-start(bf16[1,2,128,128]{3,2,1,0:T(8,128)(2,1)S(1)} %get-tuple-element.22), channel_id=1, source_target_pairs={{0,144},{48,96},{96,48},{144,0},{1,145},{49,97},{97,49},{145,1},{2... | collective-permute-start | bytes 196616 | tf_op jit(solution)/shard_map/ppermute | solution.py:182
  31.0 44.3 %collective-permute-start.6 = (bf16[2304,128]{1,0:T(8,128)(2,1)S(1)}, bf16[2304,128]{1,0:T(8,128)(2,1)}, u32[]{:S(2)}, u32[]{:S(2)}) collective-permute-start(bf16[2304,128]{1,0:T(8,128)(2,1)S(1)} %bitcast.33), channel_id=1, source_target_pairs={{0,48},{48,0},{1,49},{49,1},{2,50},{50,2},{3,51},{51,3},{4,52},{52... | collective-permute-start | bytes 1769480 | tf_op jit(solution)/shard_map/ppermute | solution.py:173
  37.6 22.1 %copy-start.4 = (bf16[4,2,128,128]{3,2,1,0:T(8,128)(2,1)}, bf16[4,2,128,128]{3,2,1,0:T(8,128)(2,1)S(1)}, u32[]{:S(2)}) copy-start(bf16[4,2,128,128]{3,2,1,0:T(8,128)(2,1)S(1)} %pad_maximum_fusion.kv_own) | copy-start | bytes 786436
  37.6 27.0 %copy-start.17 = (f32[16]{0:T(128)S(1)}, f32[16]{0:T(128)}, u32[]{:S(2)}) copy-start(f32[16]{0:T(128)} %param.15) | copy-start | bytes 196
  37.7 46.8 %copy-start.18 = (f32[128]{0:T(128)S(1)}, f32[128]{0:T(128)}, u32[]{:S(2)}) copy-start(f32[128]{0:T(128)} %param.11) | copy-start | bytes 1540
  37.7 17.7 %collective-permute-start.14 = (bf16[4,2,128,128]{3,2,1,0:T(8,128)(2,1)S(1)}, bf16[4,2,128,128]{3,2,1,0:T(8,128)(2,1)S(1)}, u32[]{:S(2)}, u32[]{:S(2)}) collective-permute-start(bf16[4,2,128,128]{3,2,1,0:T(8,128)(2,1)S(1)} %pad_maximum_fusion.kv_own), channel_id=1, source_target_pairs={{0,576},{1,577},{2,578},{3,579},{4,580},{5,581},{6,582},{7,583},{8... | collective-permute-start | bytes 786440 | tf_op jit(solution)/shard_map/ppermute | solution.py:187
  39.1 20.6 %collective-permute-start.13 = (bf16[4,2,128,128]{3,2,1,0:T(8,128)(2,1)S(1)}, bf16[4,2,128,128]{3,2,1,0:T(8,128)(2,1)}, u32[]{:S(2)}, u32[]{:S(2)}) collective-permute-start(bf16[4,2,128,128]{3,2,1,0:T(8,128)(2,1)S(1)} %pad_maximum_fusion.kv_own), channel_id=1, source_target_pairs={{0,384},{192,576},{1,385},{193,577},{2,386},{194,578},{3,387},{195... | collective-permute-start | bytes 786440 | tf_op jit(solution)/shard_map/ppermute | solution.py:187
  40.4 0.8 copy-start.1
  41.2 36.0 %collective-permute-start = (bf16[288,512]{1,0:T(8,128)(2,1)S(1)}, bf16[288,512]{1,0:T(8,128)(2,1)S(1)}, u32[]{:S(2)}, u32[]{:S(2)}) collective-permute-start(bf16[288,512]{1,0:T(8,128)(2,1)S(1)} %bitcast.38), channel_id=1, source_target_pairs={{0,1},{1,2},{2,3},{3,0},{4,5},{5,6},{6,7},{7,4},{8,9},{9,10},{10,1... | collective-permute-start | bytes 884744 | tf_op jit(solution)/shard_map/ppermute | solution.py:178
  55.3 20.0 %copy-start.16 = (bf16[4,2,128,128]{3,2,1,0:T(8,128)(2,1)}, bf16[4,2,128,128]{3,2,1,0:T(8,128)(2,1)S(1)}, u32[]{:S(2)}) copy-start(bf16[4,2,128,128]{3,2,1,0:T(8,128)(2,1)S(1)} %collective-permute-done.14.kv_three) | copy-start | bytes 786436
  55.3 24.0 %collective-permute-start.3 = (bf16[288,512]{1,0:T(8,128)(2,1)S(1)}, bf16[288,512]{1,0:T(8,128)(2,1)}, u32[]{:S(2)}, u32[]{:S(2)}) collective-permute-start(bf16[288,512]{1,0:T(8,128)(2,1)S(1)} %bitcast.36), channel_id=1, source_target_pairs={{0,3},{1,0},{2,1},{3,2},{4,7},{5,4},{6,5},{7,6},{8,11},{9,8},{10,9... | collective-permute-start | bytes 884744 | tf_op jit(solution)/shard_map/ppermute | solution.py:178
  59.7 11.2 %collective-permute-start.12 = (bf16[4,2,128,128]{3,2,1,0:T(8,128)(2,1)S(1)}, bf16[4,2,128,128]{3,2,1,0:T(8,128)(2,1)}, u32[]{:S(2)}, u32[]{:S(2)}) collective-permute-start(bf16[4,2,128,128]{3,2,1,0:T(8,128)(2,1)S(1)} %pad_maximum_fusion.kv_own), channel_id=1, source_target_pairs={{0,192},{192,384},{384,576},{1,193},{193,385},{385,577},{2,194},{1... | collective-permute-start | bytes 786440 | tf_op jit(solution)/shard_map/ppermute | solution.py:187
  61.1 31.3 %copy-start.9 = (bf16[2304,128]{1,0:T(8,128)(2,1)}, bf16[2304,128]{1,0:T(8,128)(2,1)S(1)}, u32[]{:S(2)}) copy-start(bf16[2304,128]{1,0:T(8,128)(2,1)S(1)} %collective-permute-done.7.x_far) | copy-start | bytes 1769476
  61.1 23.4 %collective-permute-start.8 = (bf16[2304,128]{1,0:T(8,128)(2,1)S(1)}, bf16[2304,128]{1,0:T(8,128)(2,1)S(1)}, u32[]{:S(2)}, u32[]{:S(2)}) collective-permute-start(bf16[2304,128]{1,0:T(8,128)(2,1)S(1)} %collective-permute-done.7.x_far), channel_id=1, source_target_pairs={{0,48},{48,0},{1,49},{49,1},{2,50},{50,2},{3,51},{51,3},{4,52},{52... | collective-permute-start | bytes 1769480 | tf_op jit(solution)/shard_map/ppermute | solution.py:173
  70.9 13.5 %collective-permute-start.2 = (bf16[288,512]{1,0:T(8,128)(2,1)S(1)}, bf16[288,512]{1,0:T(8,128)(2,1)S(1)}, u32[]{:S(2)}, u32[]{:S(2)}) collective-permute-start(bf16[288,512]{1,0:T(8,128)(2,1)S(1)} %bitcast.39), channel_id=1, source_target_pairs={{0,3},{1,0},{2,1},{3,2},{4,7},{5,4},{6,5},{7,6},{8,11},{9,8},{10,9... | collective-permute-start | bytes 884744 | tf_op jit(solution)/shard_map/ppermute | solution.py:178
  75.3 9.9 %collective-permute-start.1 = (bf16[288,512]{1,0:T(8,128)(2,1)S(1)}, bf16[288,512]{1,0:T(8,128)(2,1)S(1)}, u32[]{:S(2)}, u32[]{:S(2)}) collective-permute-start(bf16[288,512]{1,0:T(8,128)(2,1)S(1)} %bitcast.37), channel_id=1, source_target_pairs={{0,1},{1,2},{2,3},{3,0},{4,5},{5,6},{6,7},{7,4},{8,9},{9,10},{10,1... | collective-permute-start | bytes 884744 | tf_op jit(solution)/shard_map/ppermute | solution.py:178
  77.3 15.1 %copy-start.11 = (bf16[288,512]{1,0:T(8,128)(2,1)}, bf16[288,512]{1,0:T(8,128)(2,1)S(1)}, u32[]{:S(2)}) copy-start(bf16[288,512]{1,0:T(8,128)(2,1)S(1)} %collective-permute-done.w_left) | copy-start | bytes 884740
  77.3 14.3 %collective-permute-start.4 = (bf16[288,512]{1,0:T(8,128)(2,1)S(1)}, bf16[288,512]{1,0:T(8,128)(2,1)S(1)}, u32[]{:S(2)}, u32[]{:S(2)}) collective-permute-start(bf16[288,512]{1,0:T(8,128)(2,1)S(1)} %collective-permute-done.w_left), channel_id=1, source_target_pairs={{0,1},{1,2},{2,3},{3,0},{4,5},{5,6},{6,7},{7,4},{8,9},{9,10},{10,1... | collective-permute-start | bytes 884744 | tf_op jit(solution)/shard_map/ppermute | solution.py:178
  79.4 12.2 %collective-permute-start.5 = (bf16[288,512]{1,0:T(8,128)(2,1)}, bf16[288,512]{1,0:T(8,128)(2,1)S(1)}, u32[]{:S(2)}, u32[]{:S(2)}) collective-permute-start(bf16[288,512]{1,0:T(8,128)(2,1)} %collective-permute-done.3.w_right_end), channel_id=1, source_target_pairs={{0,3},{1,0},{2,1},{3,2},{4,7},{5,4},{6,5},{7,6},{8,11},{9,8},{10,9... | collective-permute-start | bytes 884744 | tf_op jit(solution)/shard_map/ppermute | solution.py:178
  84.4 7.9 %copy-start.10 = (bf16[2304,128]{1,0:T(8,128)(2,1)}, bf16[2304,128]{1,0:T(8,128)(2,1)S(1)}, u32[]{:S(2)}) copy-start(bf16[2304,128]{1,0:T(8,128)(2,1)S(1)} %collective-permute-done.8.x_both) | copy-start | bytes 1769476
  84.5 7.9 %copy-start.12 = (bf16[288,512]{1,0:T(8,128)(2,1)}, bf16[288,512]{1,0:T(8,128)(2,1)S(1)}, u32[]{:S(2)}) copy-start(bf16[288,512]{1,0:T(8,128)(2,1)S(1)} %collective-permute-done.2.w_right) | copy-start | bytes 884740
  85.2 7.2 %copy-start.13 = (bf16[288,512]{1,0:T(8,128)(2,1)}, bf16[288,512]{1,0:T(8,128)(2,1)S(1)}, u32[]{:S(2)}) copy-start(bf16[288,512]{1,0:T(8,128)(2,1)S(1)} %collective-permute-done.1.w_left_end) | copy-start | bytes 884740
  91.6 0.8 copy-start.14
  91.6 0.8 copy-start.15
  105.4 21.1 %collective-permute-start.15 = (bf16[128,512]{1,0:T(8,128)(2,1)}, bf16[128,512]{1,0:T(8,128)(2,1)S(1)}, u32[]{:S(2)}, u32[]{:S(2)}) collective-permute-start(bf16[128,512]{1,0:T(8,128)(2,1)} %get-tuple-element.10), channel_id=1, source_target_pairs={{0,48},{48,0},{96,144},{144,96},{1,49},{49,1},{97,145},{145,97},{2... | collective-permute-start | bytes 393224 | tf_op jit(solution)/shard_map/ppermute | solution.py:182
  110.0 18.7 %collective-permute-start.16 = (bf16[128,512]{1,0:T(8,128)(2,1)}, bf16[128,512]{1,0:T(8,128)(2,1)S(1)}, u32[]{:S(2)}, u32[]{:S(2)}) collective-permute-start(bf16[128,512]{1,0:T(8,128)(2,1)} %get-tuple-element.11), channel_id=1, source_target_pairs={{0,96},{48,144},{96,0},{144,48},{1,97},{49,145},{97,1},{145,49},{2... | collective-permute-start | bytes 393224 | tf_op jit(solution)/shard_map/ppermute | solution.py:182
  124.6 7.5 %collective-permute-start.17 = (bf16[128,512]{1,0:T(8,128)(2,1)}, bf16[128,512]{1,0:T(8,128)(2,1)S(1)}, u32[]{:S(2)}, u32[]{:S(2)}) collective-permute-start(bf16[128,512]{1,0:T(8,128)(2,1)} %get-tuple-element.12), channel_id=1, source_target_pairs={{0,144},{48,96},{96,48},{144,0},{1,145},{49,97},{97,49},{145,1},{2... | collective-permute-start | bytes 393224 | tf_op jit(solution)/shard_map/ppermute | solution.py:182
